TPU v7x, 32 devices: a whole 2x2x4 slice. The times are simulated.
32 devices in a mesh: kv: 8 (over z, y), tp: 4 (over x, core).
Axes of the slice: x: 2, y: 2, z: 4, core: 2. Of those that a mesh axis runs over, the one named last changes fastest.
Arguments:
- hidden_rows: bfloat16 [128, 4096], P('kv', 'tp'), may hold values from -16 to 16
- carried_state: float32 [128, 524288], P('kv', 'tp'), may hold values from -6 to 6
- norm_gain: bfloat16 [4096], replicated, may hold values from 0.099609375 to 1.8984375
- w_query: bfloat16 [4096, 2048], P('kv', 'tp'), may hold values from -0.09375 to 0.09375
- w_key: bfloat16 [4096, 2048], P('kv', 'tp'), may hold values from -0.09375 to 0.09375
- w_decay: bfloat16 [4096, 2048], P('kv', 'tp'), may hold values from -0.375 to 0.375
- w_value: bfloat16 [4096, 4096], P('kv', 'tp'), may hold values from -0.09375 to 0.09375
- w_gate: bfloat16 [4096, 4096], P('kv', 'tp'), may hold values from -0.09375 to 0.09375
- decay_bias: float32 [2048], P('tp'), may hold values from -32 to 8
- head_gain: bfloat16 [256], replicated, may hold values from 0.099609375 to 1.8984375
- w_out: bfloat16 [4096, 4096], P('tp', 'kv'), may hold values from -0.09375 to 0.09375
- mlp_gain: bfloat16 [4096], P('tp'), may hold values from 0.099609375 to 1.8984375
- w_up: bfloat16 [4096, 16384], P('tp', 'kv'), may hold values from -0.09375 to 0.09375
- w_down: bfloat16 [16384, 4096], P('kv', 'tp'), may hold values from -0.046875 to 0.046875
Outputs:
- updated_rows: bfloat16 [128, 4096], P('kv', 'tp')
- new_state: float32 [128, 524288], P('kv', 'tp')
All inputs are finite; a program needn't handle non-finite values.
Results may differ from a plain program's by a relative error of at most 0.025.
Values may be sent and summed in bfloat16 or wider, within the bound.
A program may use at most 128 MiB of HBM per device.

v0:
```python
import functools

import jax
import jax.numpy as jnp
from jax import lax
from jax.experimental import pallas as pl
from jax.experimental.pallas import tpu as pltpu
from jax.sharding import PartitionSpec as P

DK = 128
DV = 256

epsilon = 1e-06
decay_normalizer = 16.0

F32 = jnp.float32
BF16 = jnp.bfloat16
MESH = pl.DeviceIdType.MESH


def remote(src, dst, send_sem, recv_sem, i, j):
    return pltpu.make_async_remote_copy(
        src_ref=src,
        dst_ref=dst,
        send_sem=send_sem,
        recv_sem=recv_sem,
        device_id={"kv": i, "tp": j},
        device_id_type=MESH,
    )


def dot(a, b):
    return jnp.dot(a, b, preferred_element_type=F32)


def inner_size(kv):
    size = 1
    while (size * 2) ** 2 <= kv:
        size = size * 2
    return size


def project_kernel(
    kv, tp, h_ref, g_ref, w0, w1, w2, w3, w4, o0, o1, o2, o3, o4,
    xbuf, v0, v1, v2, v3, v4, s0, s1, s2, s3, s4, r0, r1, r2, r3, r4,
    t0, t1, t2, t3, t4, u0, u1, u2, u3, u4,
    ssq, wsem, xs_sem, xr_sem, ss_sem, sr_sem, ps_sem, pr_sem, qs_sem, qr_sem,
):
    i, j = lax.axis_index("kv"), lax.axis_index("tp")
    ny = inner_size(kv)
    nz = kv // ny
    z, y = i // ny, lax.rem(i, ny)
    ratio = kv // tp
    rows = h_ref.shape[0]
    width = xbuf.shape[2]
    owner = i // ratio
    ws, vs, outs = (w0, w1, w2, w3, w4), (v0, v1, v2, v3, v4), (o0, o1, o2, o3, o4)
    sends, recvs = (s0, s1, s2, s3, s4), (r0, r1, r2, r3, r4)
    sums, finals = (t0, t1, t2, t3, t4), (u0, u1, u2, u3, u4)
    order = (3, 4, 1, 0, 2)
    loads = [pltpu.make_async_copy(w, v, wsem.at[n]) for n, (w, v) in enumerate(zip(ws, vs))]

    hidden_sends = []
    for a in range(ratio):
        for s in range(tp):
            dst_i, dst_j = j * ratio + a, lax.rem(j + s, tp)
            src = h_ref.at[:, pl.ds(a * width, width)]
            copy = remote(
                src, xbuf.at[i], xs_sem.at[a * tp + s], xr_sem.at[i], dst_i, dst_j
            )
            hidden_sends.append((a, s, dst_i, copy))
    for a, s, dst_i, copy in hidden_sends:
        if s:
            copy.start()
        else:
            pl.when(dst_i != i)(copy.start)
    for n in order:
        loads[n].start()

    hidden = h_ref[...].astype(F32)
    ssq[j] = jnp.broadcast_to(jnp.sum(hidden * hidden, axis=1, keepdims=True), (rows, 128))
    for a, s, dst_i, copy in hidden_sends:
        if not s:

            @pl.when(dst_i == i)
            def _():
                xbuf[i] = h_ref[:, a * width : (a + 1) * width]

    for s in range(kv):
        k = lax.rem(i + s, kv)
        arrive = remote(xbuf.at[k], xbuf.at[k], xs_sem.at[0], xr_sem.at[k], k, owner)
        if s:
            arrive.wait_recv()
        else:
            pl.when(owner != j)(arrive.wait_recv)

    square_sends = [
        remote(ssq.at[j], ssq.at[j], ss_sem.at[s], sr_sem.at[j], i, lax.rem(j + s, tp))
        for s in range(1, tp)
    ]
    gain = g_ref[:, pl.ds(pl.multiple_of(i * width, 128), width)].astype(F32)
    x = (xbuf[...].reshape(kv * rows, width).astype(F32) * gain).astype(BF16)
    part_sends = []
    for n in order:
        loads[n].wait()
        part = dot(x, vs[n][...]).astype(BF16)
        for zz in range(nz):
            for yy in range(ny):
                low = (zz * ny + yy) * rows
                sends[n][yy, zz] = part[low : low + rows]
        for s in range(1, ny):
            yy = lax.rem(y + s, ny)
            copy = remote(
                sends[n].at[yy], recvs[n].at[y], ps_sem.at[n, s], pr_sem.at[n, y], z * ny + yy, j
            )
            copy.start()
            part_sends.append(copy)
    for copy in square_sends:
        copy.start()
    for n in order:
        acc = sends[n][y].astype(F32)
        for s in range(1, ny):
            yy = lax.rem(y + s, ny)
            remote(
                recvs[n].at[yy], recvs[n].at[yy], ps_sem.at[n, 0], pr_sem.at[n, yy], z * ny + yy, j
            ).wait_recv()
            acc = acc + recvs[n][yy].astype(F32)
        sums[n][...] = acc.astype(BF16)
        for s in range(1, nz):
            zz = lax.rem(z + s, nz)
            copy = remote(
                sums[n].at[zz], finals[n].at[z], qs_sem.at[n, s], qr_sem.at[n, z], zz * ny + y, j
            )
            copy.start()
            part_sends.append(copy)
    for s in range(1, tp):
        k = lax.rem(j + s, tp)
        remote(ssq.at[k], ssq.at[k], ss_sem.at[0], sr_sem.at[k], i, k).wait_recv()
    total = ssq[0]
    for s in range(1, tp):
        total = total + ssq[s]
    scale = lax.rsqrt(total[:, :1] / (kv * width) + epsilon)
    for n in order:
        acc = sums[n][z].astype(F32)
        for s in range(1, nz):
            zz = lax.rem(z + s, nz)
            remote(
                finals[n].at[zz], finals[n].at[zz], qs_sem.at[n, 0], qr_sem.at[n, zz], zz * ny + y, j
            ).wait_recv()
            acc = acc + finals[n][zz].astype(F32)
        outs[n][...] = (acc * scale).astype(BF16)
    for a, s, dst_i, copy in hidden_sends:
        if s:
            copy.wait_send()
        else:
            pl.when(dst_i != i)(copy.wait_send)
    for copy in square_sends + part_sends:
        copy.wait_send()


def project(kv, tp, hidden_rows, norm_gain, weights):
    rows = hidden_rows.shape[0]
    width = weights[0].shape[0]
    ny = inner_size(kv)
    nz = kv // ny
    vmem = pl.BlockSpec(memory_space=pltpu.VMEM)
    anywhere = pl.BlockSpec(memory_space=pl.ANY)
    slots = [pltpu.VMEM((ny, nz, rows, w.shape[1]), BF16) for w in weights]
    lines = [pltpu.VMEM((nz, rows, w.shape[1]), BF16) for w in weights]
    dma = pltpu.SemaphoreType.DMA
    return pl.pallas_call(
        functools.partial(project_kernel, kv, tp),
        out_shape=[jax.ShapeDtypeStruct((rows, w.shape[1]), BF16) for w in weights],
        in_specs=[vmem] * 2 + [anywhere] * 5,
        out_specs=[vmem] * 5,
        scratch_shapes=[pltpu.VMEM((kv, rows, width), BF16)]
        + [pltpu.VMEM(w.shape, BF16) for w in weights]
        + slots
        + slots
        + lines
        + lines
        + [
            pltpu.VMEM((tp, rows, 128), F32),
            dma((5,)),
            dma((kv,)),
            dma((kv,)),
            dma((tp,)),
            dma((tp,)),
            dma((5, ny)),
            dma((5, ny)),
            dma((5, nz)),
            dma((5, nz)),
        ],
        compiler_params=pltpu.CompilerParams(
            has_side_effects=True, vmem_limit_bytes=62 * 1024 * 1024
        ),
        name="project",
    )(hidden_rows, norm_gain.reshape(1, -1), *weights)


PARTS = 2
CHUNKS = 4


def state_kernel(
    q_ref, k_ref, d_ref, v_ref, g_ref, bias_ref, gain_ref, old_ref, new_ref, mixed_ref,
    query, key, decay, total,
):
    part = pl.program_id(1)
    channels = DK // PARTS

    @pl.when(part == 0)
    def _():
        pre = d_ref[...].astype(F32) + bias_ref[...]
        log_decay = jnp.minimum(pre, 0.0) - jnp.log1p(jnp.exp(-jnp.abs(pre)))
        decay[...] = jnp.exp(log_decay / decay_normalizer)
        query[...] = q_ref[...].astype(F32) * DK ** (-0.5)
        key[...] = k_ref[...].astype(F32)
        total[...] = jnp.zeros_like(total)

    value = v_ref[...].astype(F32)
    acc = total[...]
    q, k, d = query[...], key[...], decay[...]
    for c in range(channels):
        at = slice(c * DV, (c + 1) * DV)
        new = d[:, c : c + 1] * old_ref[:, at] + k[:, c : c + 1] * value
        new_ref[:, at] = new
        acc = acc + q[:, c : c + 1] * new
    total[...] = acc
    query[...] = pltpu.roll(q, DK - channels, 1)
    key[...] = pltpu.roll(k, DK - channels, 1)
    decay[...] = pltpu.roll(d, DK - channels, 1)

    @pl.when(part == PARTS - 1)
    def _():
        gate = g_ref[...].astype(F32)
        mixed = acc * lax.rsqrt(jnp.mean(acc * acc, axis=1, keepdims=True) + epsilon)
        mixed_ref[...] = (mixed * gain_ref[...].astype(F32) * jax.nn.silu(gate)).astype(BF16)


def state(queries, keys_new, decay_pre, values, out_gate, decay_bias, head_gain, carried):
    rows, total = carried.shape
    heads = total // (DK * DV)
    narrow = pl.BlockSpec((rows, DK), lambda h, p: (0, h))
    wide = pl.BlockSpec((rows, DV), lambda h, p: (0, h))
    block = pl.BlockSpec((rows, DK * DV // PARTS), lambda h, p: (0, h * PARTS + p))
    return pl.pallas_call(
        state_kernel,
        grid=(heads, PARTS),
        out_shape=[
            jax.ShapeDtypeStruct(carried.shape, F32),
            jax.ShapeDtypeStruct((rows, heads * DV), BF16),
        ],
        in_specs=[narrow] * 3
        + [wide] * 2
        + [
            pl.BlockSpec((1, DK), lambda h, p: (0, h)),
            pl.BlockSpec((1, DV), lambda h, p: (0, 0)),
            block,
        ],
        out_specs=[block, wide],
        scratch_shapes=[pltpu.VMEM((rows, DK), F32)] * 3 + [pltpu.VMEM((rows, DV), F32)],
        compiler_params=pltpu.CompilerParams(vmem_limit_bytes=62 * 1024 * 1024),
        name="state",
    )(
        queries, keys_new, decay_pre, values, out_gate,
        decay_bias.reshape(1, -1), head_gain.reshape(1, -1), carried,
    )


def tail_kernel(
    kv, tp, mixed_ref, h_ref, g_ref, wo, wu, wd, out_ref,
    vo, vu, vd, mall, psend, precv, resid, rall, ssq, usend, urecv, xsend, xrecv, act, dsend, drecv,
    wsem, ms_sem, mr_sem, ps_sem, pr_sem, rs_sem, rr_sem, ss_sem, sr_sem,
    us_sem, ur_sem, xs_sem, xr_sem, as_sem, ar_sem, ds_sem, dr_sem,
):
    i, j = lax.axis_index("kv"), lax.axis_index("tp")
    ratio = kv // tp
    rows, columns = h_ref.shape
    width = columns // ratio
    owner = i // ratio
    loads = [
        pltpu.make_async_copy(w, v, wsem.at[n])
        for n, (w, v) in enumerate(((wo, vo), (wu, vu), (wd, vd)))
    ]
    sent = []

    def everyone(src_of, dst, send_sem, recv_sem):
        for s in range(1, kv):
            k = lax.rem(i + s, kv)
            copy = remote(src_of(k), dst.at[i], send_sem.at[s], recv_sem.at[i], k, j)
            copy.start()
            sent.append(copy)

    def arrived(dst, send_sem, recv_sem, s):
        k = lax.rem(i + s, kv)
        remote(dst.at[k], dst.at[k], send_sem.at[0], recv_sem.at[k], k, j).wait_recv()
        return k

    everyone(lambda k: mixed_ref, mall, ms_sem, mr_sem)
    for load in loads:
        load.start()
    mall[i] = mixed_ref[...]
    for s in range(1, kv):
        arrived(mall, ms_sem, mr_sem, s)
    loads[0].wait()
    part = dot(mall[...].reshape(kv * rows, mall.shape[2]), vo[...]).astype(BF16)
    psend[...] = part.reshape(psend.shape)

    slot = j * ratio + lax.rem(i, ratio)
    own_send = remote(psend.at[i], precv.at[slot], ps_sem.at[0], pr_sem.at[slot], i, owner)
    for s in range(1, kv):
        k = lax.rem(i + s, kv)
        copy = remote(psend.at[k], precv.at[slot], ps_sem.at[s], pr_sem.at[slot], k, owner)
        copy.start()
        sent.append(copy)
    pl.when(owner != j)(own_send.start)

    @pl.when(owner == j)
    def _():
        precv[slot] = psend[i]

    pieces = []
    for a in range(ratio):
        src_i = j * ratio + a
        attn = None
        for s in range(tp):
            src_j = lax.rem(j + s, tp)
            at = src_j * ratio + a
            arrive = remote(precv.at[at], precv.at[at], ps_sem.at[0], pr_sem.at[at], src_i, src_j)
            if s:
                arrive.wait_recv()
            else:
                pl.when(src_i != i)(arrive.wait_recv)
            term = precv[at].astype(F32)
            attn = term if attn is None else attn + term
        hidden = h_ref[:, a * width : (a + 1) * width].astype(F32)
        piece = (hidden + attn.astype(BF16).astype(F32)).astype(BF16)
        resid[:, a * width : (a + 1) * width] = piece
        piece = piece.astype(F32)
        pieces.append(jnp.sum(piece * piece, axis=1, keepdims=True))

    everyone(lambda k: resid, rall, rs_sem, rr_sem)
    ssq[j] = jnp.broadcast_to(sum(pieces), (rows, 128))
    rall[i] = resid[...]
    loads[1].wait()
    for s in range(1, kv):
        arrived(rall, rs_sem, rr_sem, s)
    for s in range(1, tp):
        copy = remote(ssq.at[j], ssq.at[j], ss_sem.at[s], sr_sem.at[j], i, lax.rem(j + s, tp))
        copy.start()
        sent.append(copy)
    x = (rall[...].reshape(kv * rows, columns).astype(F32) * g_ref[...].astype(F32)).astype(BF16)

    half = vu.shape[1] // 2
    chunks = usend.shape[0]
    piece = half // chunks
    core, across = lax.rem(j, 2), j // 2
    other = 1 - core
    partner = across * 2 + other

    def columns_of(h, c):
        return pl.ds(pl.multiple_of(h * half + c * piece, 128), piece)

    def give(c):
        usend[c] = dot(x, vu[:, columns_of(other, c)]).astype(BF16)
        copy = remote(usend.at[c], urecv.at[c], us_sem.at[c], ur_sem.at[c], i, partner)
        copy.start()
        sent.append(copy)

    give(0)
    for c in range(chunks):
        if c + 1 < chunks:
            give(c + 1)
        mine = dot(x, vu[:, columns_of(core, c)])
        remote(urecv.at[c], urecv.at[c], us_sem.at[c], ur_sem.at[c], i, partner).wait_recv()
        xsend[c] = (mine + urecv[c].astype(F32)).astype(BF16)
        for s in range(1, tp // 2):
            to = lax.rem(across + s, tp // 2)
            copy = remote(
                xsend.at[c],
                xrecv.at[across, c],
                xs_sem.at[s, c],
                xr_sem.at[across, c],
                i,
                to * 2 + core,
            )
            copy.start()
            sent.append(copy)
    loads[2].wait()
    down = None
    for c in range(chunks):
        total = xsend[c].astype(F32)
        for s in range(1, tp // 2):
            at = lax.rem(across + s, tp // 2)
            slot_ref = xrecv.at[at, c]
            remote(
                slot_ref, slot_ref, xs_sem.at[0, c], xr_sem.at[at, c], i, at * 2 + core
            ).wait_recv()
            total = total + xrecv[at, c].astype(F32)
        act[core, c] = jnp.square(jnp.maximum(total, 0.0)).astype(BF16)
        copy = remote(
            act.at[core, c], act.at[core, c], as_sem.at[c], ar_sem.at[core, c], i, partner
        )
        copy.start()
        sent.append(copy)
        term = dot(act[core, c], vd[columns_of(core, c), :])
        down = term if down is None else down + term
        arrive = act.at[other, c]
        remote(arrive, arrive, as_sem.at[c], ar_sem.at[other, c], i, partner).wait_recv()
        down = down + dot(act[other, c], vd[columns_of(other, c), :])
    dsend[...] = down.astype(BF16).reshape(dsend.shape)
    everyone(lambda k: dsend.at[k], drecv, ds_sem, dr_sem)

    for s in range(1, tp):
        k = lax.rem(j + s, tp)
        remote(ssq.at[k], ssq.at[k], ss_sem.at[0], sr_sem.at[k], i, k).wait_recv()
    squares = ssq[0]
    for s in range(1, tp):
        squares = squares + ssq[s]
    scale = lax.rsqrt(squares[:, :1] / (columns * tp) + epsilon)
    acc = dsend[i].astype(F32)
    for s in range(1, kv):
        k = arrived(drecv, ds_sem, dr_sem, s)
        acc = acc + drecv[k].astype(F32)
    acc = (acc * (scale * scale)).astype(BF16)
    out_ref[...] = (resid[...].astype(F32) + acc.astype(F32)).astype(BF16)
    pl.when(owner != j)(own_send.wait_send)
    for copy in sent:
        copy.wait_send()


def tail(kv, tp, mixed, hidden_rows, mlp_gain, w_out, w_up, w_down):
    rows, columns = hidden_rows.shape
    width = w_out.shape[1]
    ratio = kv // tp
    half = w_up.shape[1] // 2
    everything = kv * rows
    chunks = max(1, min(CHUNKS, half // 128))
    vmem = pl.BlockSpec(memory_space=pltpu.VMEM)
    anywhere = pl.BlockSpec(memory_space=pl.ANY)
    dma = pltpu.SemaphoreType.DMA
    return pl.pallas_call(
        functools.partial(tail_kernel, kv, tp),
        out_shape=jax.ShapeDtypeStruct((rows, columns), BF16),
        in_specs=[vmem] * 3 + [anywhere] * 3,
        out_specs=vmem,
        scratch_shapes=[
            pltpu.VMEM(w_out.shape, BF16),
            pltpu.VMEM(w_up.shape, BF16),
            pltpu.VMEM(w_down.shape, BF16),
            pltpu.VMEM((kv, rows, mixed.shape[1]), BF16),
            pltpu.VMEM((kv, rows, width), BF16),
            pltpu.VMEM((tp * ratio, rows, width), BF16),
            pltpu.VMEM((rows, columns), BF16),
            pltpu.VMEM((kv, rows, columns), BF16),
            pltpu.VMEM((tp, rows, 128), F32),
            pltpu.VMEM((chunks, everything, half // chunks), BF16),
            pltpu.VMEM((chunks, everything, half // chunks), BF16),
            pltpu.VMEM((chunks, everything, half // chunks), BF16),
            pltpu.VMEM((tp // 2, chunks, everything, half // chunks), BF16),
            pltpu.VMEM((2, chunks, everything, half // chunks), BF16),
            pltpu.VMEM((kv, rows, columns), BF16),
            pltpu.VMEM((kv, rows, columns), BF16),
            dma((3,)),
            dma((kv,)),
            dma((kv,)),
            dma((kv,)),
            dma((tp * ratio,)),
            dma((kv,)),
            dma((kv,)),
            dma((tp,)),
            dma((tp,)),
            dma((chunks,)),
            dma((chunks,)),
            dma((tp // 2, chunks)),
            dma((tp // 2, chunks)),
            dma((chunks,)),
            dma((2, chunks)),
            dma((kv,)),
            dma((kv,)),
        ],
        compiler_params=pltpu.CompilerParams(
            has_side_effects=True, vmem_limit_bytes=62 * 1024 * 1024
        ),
        name="tail",
    )(mixed, hidden_rows, mlp_gain.reshape(1, -1), w_out, w_up, w_down)


def body(
    kv,
    tp,
    hidden_rows,
    carried_state,
    norm_gain,
    w_query,
    w_key,
    w_decay,
    w_value,
    w_gate,
    decay_bias,
    head_gain,
    w_out,
    mlp_gain,
    w_up,
    w_down,
):
    queries, keys_new, decay_pre, values, out_gate = project(
        kv, tp, hidden_rows, norm_gain, (w_query, w_key, w_decay, w_value, w_gate)
    )
    new_state, mixed = state(
        queries, keys_new, decay_pre, values, out_gate, decay_bias, head_gain, carried_state
    )
    updated_rows = tail(kv, tp, mixed, hidden_rows, mlp_gain, w_out, w_up, w_down)
    return (updated_rows, new_state)


def solution(mesh):
    return jax.shard_map(
        functools.partial(body, mesh.shape["kv"], mesh.shape["tp"]),
        mesh=mesh,
        in_specs=(
            P("kv", "tp"),
            P("kv", "tp"),
            P(),
            P("kv", "tp"),
            P("kv", "tp"),
            P("kv", "tp"),
            P("kv", "tp"),
            P("kv", "tp"),
            P("tp"),
            P(),
            P("tp", "kv"),
            P("tp"),
            P("tp", "kv"),
            P("kv", "tp"),
        ),
        out_specs=(P("kv", "tp"), P("kv", "tp")),
        check_vma=False,
    )
```

profile of v0, /device:TPU:0, one launch (start us, length us, event | category | flops | bytes accessed | tf_op | source)
XLA Modules:
  0.0 94.5 jit_solution(11847631513680989599)
XLA Ops:
  0.6 0.0 copy-start
  0.6 1.3 %reshape.16.g_ref = bf16[1,4096]{1,0:T(2,128)(2,1)} reshape(bf16[4096]{0:T(1024)(128)(2,1)} %param.16) | data formatting | bytes 16384 | tf_op jit(solution)/shard_map/reshape | solution.py:198
  2.0 35.8 %project.1 = (bf16[16,512]{1,0:T(8,128)(2,1)}, bf16[16,512]{1,0:T(8,128)(2,1)}, bf16[16,512]{1,0:T(8,128)(2,1)}, bf16[16,1024]{1,0:T(8,128)(2,1)}, bf16[16,1024]{1,0:T(8,128)(2,1)}) custom-call(bf16[16,1024]{1,0:T(8,128)(2,1)} %h_ref.3, bf16[1,4096]{1,0:T(2,128)(2,1)} %reshape.16.g_ref, bf16[512,512]{1,0:T(8,128)(2,1)} %w0.1, bf16[512,512]{1,0:T(8,128)(2,1)} %w1.1, ...), custom_call_target="tpu_custom_call" | custom-call | tf_op jit(solution)/shard_map/project/pallas_call | solution.py:171
  37.8 1.2 %reshape.18.gain_ref = bf16[1,256]{1,0:T(2,128)(2,1)} reshape(bf16[256]{0:T(256)(128)(2,1)} %param.23) | data formatting | bytes 1024 | tf_op jit(solution)/shard_map/reshape | solution.py:267
  39.0 10.7 %state.1 = (f32[16,131072]{1,0:T(8,128)}, bf16[16,1024]{1,0:T(8,128)(2,1)}) custom-call(bf16[16,512]{1,0:T(8,128)(2,1)} %get-tuple-element.9.q_ref, bf16[16,512]{1,0:T(8,128)(2,1)} %get-tuple-element.10.k_ref, bf16[16,512]{1,0:T(8,128)(2,1)} %get-tuple-element.11.d_ref, bf16[16,1024]{1,0:T(8,128)(2,1)} %get-tuple-element.12.v_ref, ...), custom_call_target="tpu_custom_call" | custom-call | tf_op jit(solution)/shard_map/state/pallas_call | solution.py:247
  49.7 0.0 copy-done
  49.7 0.6 reshape.19.g_ref
  50.3 42.8 %tail.1 = bf16[16,1024]{1,0:T(8,128)(2,1)} custom-call(bf16[16,1024]{1,0:T(8,128)(2,1)} %get-tuple-element.14.mixed_ref, bf16[16,1024]{1,0:T(8,128)(2,1)} %h_ref.3, bf16[1,1024]{1,0:T(2,128)(2,1)} %reshape.19.g_ref, bf16[1024,512]{1,0:T(8,128)(2,1)} %wo.1, bf16[1024,2048]{1,0:T(8,128)(2,1)} %wu.1, bf16[2048,1024]{1,0:T(8,128)(2,1)} %wd.1), custom_call_target="tpu_custom_call" | custom-call | tf_op jit(solution)/shard_map/tail/pallas_call | solution.py:443
  93.1 1.4 %copy.17 = bf16[16,1024]{1,0:T(8,128)(2,1)} copy(bf16[16,1024]{1,0:T(8,128)(2,1)} %tail.1) | data formatting | bytes 65536
Async XLA Ops:
  0.6 49.1 %copy-start = (bf16[1024]{0:T(1024)(128)(2,1)S(1)}, bf16[1024]{0:T(1024)(128)(2,1)}, u32[]{:S(2)}) copy-start(bf16[1024]{0:T(1024)(128)(2,1)} %param.25) | copy-start | bytes 6148
where the time goes:
time: 95.1 us; the launch traced here: 94.5 us
  Pallas kernels  89.3 us (94%)
  local copies, waits for them, and re-layouts  4.51 us (5%)
    pallas_call x1, Pallas kernels, tail(): pl.pallas_call(functools.partial(tail_kernel, kv, tp), out_shape=jax.Shap...  42.8 us
    pallas_call x1, Pallas kernels, project(): pl.pallas_call(functools.partial(project_kernel, kv, tp), out_shape=[jax....  35.8 us
    pallas_call x1, Pallas kernels, state(): pl.pallas_call(state_kernel, grid=(heads, PARTS), out_shape=[jax.ShapeDty...  10.7 us

commit v1 on v0

v1 whole, which is shorter than its diff:
```python
import functools

import jax
import jax.numpy as jnp
from jax import lax
from jax.experimental import pallas as pl
from jax.experimental.pallas import tpu as pltpu
from jax.sharding import PartitionSpec as P

DK = 128
DV = 256

epsilon = 1e-06
decay_normalizer = 16.0

F32 = jnp.float32
BF16 = jnp.bfloat16
MESH = pl.DeviceIdType.MESH
CHUNKS = 4
VMEM_BYTES = 67043328


def remote(src, dst, send_sem, recv_sem, i, j):
    return pltpu.make_async_remote_copy(
        src_ref=src,
        dst_ref=dst,
        send_sem=send_sem,
        recv_sem=recv_sem,
        device_id={"kv": i, "tp": j},
        device_id_type=MESH,
    )


def dot(a, b):
    return jnp.dot(a, b, preferred_element_type=F32)


def inner_size(kv):
    size = 1
    while (size * 2) ** 2 <= kv:
        size = size * 2
    return size


def layer_kernel(
    kv, tp,
    h_ref, ng_ref, bias_ref, hg_ref, mg_ref, wq, wk, wd_, wv, wg, old, wo, wu, wdn,
    out_ref, st_ref,
    vq, vk, vd_, vv, vg, vo, vu, vdn,
    xbuf, psnd, prcv, zsnd, zrcv, ssq, query, key, decay, value, head,
    mixed, mall, asend, arecv, rpart, rall, usend, urecv, xsend, xrecv, act, dsend, drecv, ssq2,
    wsem, stsem, hs_sem, hr_sem, ss_sem, sr_sem, ps_sem, pr_sem, qs_sem, qr_sem,
    ms_sem, mr_sem, as_sem, ar_sem, rs_sem, rr_sem, ts_sem, tr_sem,
    us_sem, ur_sem, xs_sem, xr_sem, cs_sem, cr_sem, ds_sem, dr_sem,
):
    i, j = lax.axis_index("kv"), lax.axis_index("tp")
    ny = inner_size(kv)
    nz = kv // ny
    z, y = i // ny, lax.rem(i, ny)
    ratio = kv // tp
    owner = i // ratio
    rows = h_ref.shape[0]
    columns = h_ref.shape[1]
    width = xbuf.shape[2]
    cw = vq.shape[1]
    heads = cw // DK
    sent = []

    def start(copy):
        copy.start()
        sent.append((copy, None))

    def start_if(condition, copy):
        pl.when(condition)(copy.start)
        sent.append((copy, condition))

    barrier = pltpu.get_barrier_semaphore()

    def greet(a, b):
        pl.semaphore_signal(
            barrier, inc=1, device_id={"kv": a, "tp": b}, device_id_type=MESH
        )

    for s in range(kv):
        k = lax.rem(i + s, kv)
        if s:
            greet(k, owner)
            greet(k, j)
        else:
            pl.when(owner != j)(lambda: greet(i, owner))
    for a in range(ratio):
        for s in range(tp):
            k, t = j * ratio + a, lax.rem(j + s, tp)
            if s:
                greet(k, t)
            else:
                pl.when(k != i)(functools.partial(greet, k, t))
    for s in range(1, tp):
        greet(i, lax.rem(j + s, tp))

    loads = [
        pltpu.make_async_copy(w, v, wsem.at[n])
        for n, (w, v) in enumerate(
            ((wd_, vd_), (wk, vk), (wq, vq), (wv, vv), (wg, vg), (wo, vo), (wu, vu), (wdn, vdn))
        )
    ]
    load_state = pltpu.make_async_copy(old, st_ref, stsem)
    for load in loads[:5]:
        load.start()
    load_state.start()
    for load in loads[5:]:
        load.start()

    hidden = h_ref[...].astype(F32)
    ssq[j] = jnp.broadcast_to(jnp.sum(hidden * hidden, axis=1, keepdims=True), (rows, 128))
    itself = jnp.where(owner == j, 1, 0)
    pl.semaphore_wait(barrier, 2 * (kv - itself) + (kv - 1) + (tp - 1))

    for a in range(ratio):
        for s in range(tp):
            k, t = j * ratio + a, lax.rem(j + s, tp)
            copy = remote(
                h_ref.at[:, pl.ds(a * width, width)], xbuf.at[i],
                hs_sem.at[a * tp + s], hr_sem.at[i], k, t,
            )
            if s:
                start(copy)
            else:
                start_if(k != i, copy)

                @pl.when(k == i)
                def _():
                    xbuf[i] = h_ref[:, a * width : (a + 1) * width]

    for s in range(1, tp):
        start(remote(ssq.at[j], ssq.at[j], ss_sem.at[s], sr_sem.at[j], i, lax.rem(j + s, tp)))

    gain = ng_ref[:, pl.ds(pl.multiple_of(i * width, 128), width)].astype(F32)
    for s in range(kv):
        k = lax.rem(i + s, kv)
        arrive = remote(xbuf.at[k], xbuf.at[k], hs_sem.at[0], hr_sem.at[k], k, owner)
        if s:
            arrive.wait_recv()
        else:
            pl.when(owner != j)(arrive.wait_recv)
    x = (xbuf[...].reshape(kv * rows, width).astype(F32) * gain).astype(BF16)

    pieces = []
    for n, v in enumerate((vd_, vk, vq, vv, vg)):
        for low in range(0, v.shape[1], cw):
            pieces.append((n, v, low))
    for c, (n, v, low) in enumerate(pieces):
        if low == 0:
            loads[n].wait()
        part = dot(x, v[:, low : low + cw]).astype(BF16)
        for zz in range(nz):
            for yy in range(ny):
                at = (zz * ny + yy) * rows
                psnd[c, yy, zz] = part[at : at + rows]
        for s in range(1, ny):
            yy = lax.rem(y + s, ny)
            start(
                remote(
                    psnd.at[c, yy], prcv.at[c, y], ps_sem.at[c, s], pr_sem.at[c, y], z * ny + yy, j
                )
            )

    def along_z(c):
        acc = psnd[c, y].astype(F32)
        for s in range(1, ny):
            yy = lax.rem(y + s, ny)
            at = prcv.at[c, yy]
            remote(at, at, ps_sem.at[c, 0], pr_sem.at[c, yy], z * ny + yy, j).wait_recv()
            acc = acc + prcv[c, yy].astype(F32)
        zsnd[c] = acc.astype(BF16)
        for s in range(1, nz):
            zz = lax.rem(z + s, nz)
            start(
                remote(
                    zsnd.at[c, zz], zrcv.at[c, z], qs_sem.at[c, s], qr_sem.at[c, z], zz * ny + y, j
                )
            )

    def reduced(c):
        acc = zsnd[c, z].astype(F32)
        for s in range(1, nz):
            zz = lax.rem(z + s, nz)
            at = zrcv.at[c, zz]
            remote(at, at, qs_sem.at[c, 0], qr_sem.at[c, zz], zz * ny + y, j).wait_recv()
            acc = acc + zrcv[c, zz].astype(F32)
        return (acc * scale).astype(BF16).astype(F32)

    for c in range(len(pieces)):
        along_z(c)
    for s in range(1, tp):
        k = lax.rem(j + s, tp)
        remote(ssq.at[k], ssq.at[k], ss_sem.at[0], sr_sem.at[k], i, k).wait_recv()
    total = ssq[0]
    for s in range(1, tp):
        total = total + ssq[s]
    scale = lax.rsqrt(total[:, :1] / (kv * width) + epsilon)

    pre = reduced(0) + bias_ref[...]
    log_decay = jnp.minimum(pre, 0.0) - jnp.log1p(jnp.exp(-jnp.abs(pre)))
    decay[...] = jnp.exp(log_decay / decay_normalizer)
    key[...] = reduced(1)
    query[...] = reduced(2) * DK ** (-0.5)
    for c in range(3, 5):
        value[:, (c - 3) * cw : (c - 2) * cw] = reduced(c)
    load_state.wait()

    @pl.loop(0, heads)
    def _(h):
        narrow = pl.ds(pl.multiple_of(h * DK, DK), DK)
        wide = pl.ds(pl.multiple_of(h * DV, DV), DV)
        q, k, d = query[:, narrow], key[:, narrow], decay[:, narrow]
        v = value[:, wide]
        acc = jnp.zeros((rows, DV), F32)
        for c in range(DK):
            at = pl.ds(pl.multiple_of(h * (DK * DV) + c * DV, DV), DV)
            new = d[:, c : c + 1] * st_ref[:, at] + k[:, c : c + 1] * v
            st_ref[:, at] = new
            acc = acc + q[:, c : c + 1] * new
        acc = acc * lax.rsqrt(jnp.mean(acc * acc, axis=1, keepdims=True) + epsilon)
        head[:, wide] = acc * hg_ref[...].astype(F32)

    for c in range(5, 7):
        at = slice((c - 5) * cw, (c - 4) * cw)
        mixed[:, at] = (head[:, at] * jax.nn.silu(reduced(c))).astype(BF16)

    def everyone(src_of, dst, send_sem, recv_sem):
        for s in range(1, kv):
            k = lax.rem(i + s, kv)
            start(remote(src_of(k), dst.at[i], send_sem.at[s], recv_sem.at[i], k, j))

    def arrived(dst, send_sem, recv_sem, s):
        k = lax.rem(i + s, kv)
        remote(dst.at[k], dst.at[k], send_sem.at[0], recv_sem.at[k], k, j).wait_recv()
        return k

    everyone(lambda k: mixed, mall, ms_sem, mr_sem)
    mall[i] = mixed[...]
    loads[5].wait()
    for s in range(1, kv):
        arrived(mall, ms_sem, mr_sem, s)
    part = dot(mall[...].reshape(kv * rows, mall.shape[2]), vo[...]).astype(BF16)
    asend[...] = part.reshape(asend.shape)
    for s in range(1, tp):
        t = lax.rem(j + s, tp)
        start(remote(asend.at[t], arecv.at[j], as_sem.at[s], ar_sem.at[j], i, t))
    attn = asend[j].astype(F32)
    for s in range(1, tp):
        t = lax.rem(j + s, tp)
        remote(arecv.at[t], arecv.at[t], as_sem.at[0], ar_sem.at[t], i, t).wait_recv()
        attn = attn + arecv[t].astype(F32)
    mine = xbuf[pl.ds(j * ratio, ratio)].reshape(ratio * rows, width).astype(F32)
    rpart[...] = (mine + attn.astype(BF16).astype(F32)).astype(BF16)

    slot = lax.rem(i, ratio)
    for s in range(kv):
        k = lax.rem(i + s, kv)
        copy = remote(rpart, rall.at[slot, j], rs_sem.at[s], rr_sem.at[slot, j], k, owner)
        if s:
            start(copy)
        else:
            start_if(owner != j, copy)

    @pl.when(owner == j)
    def _():
        rall[slot, j] = rpart[...]

    loads[6].wait()
    for a in range(ratio):
        k = j * ratio + a
        for s in range(tp):
            t = lax.rem(j + s, tp)
            at = rall.at[a, t]
            arrive = remote(at, at, rs_sem.at[0], rr_sem.at[a, t], k, t)
            if s:
                arrive.wait_recv()
            else:
                pl.when(k != i)(arrive.wait_recv)

    def own(a):
        return rall[a, owner, pl.ds(pl.multiple_of(slot * rows, rows), rows), :]

    squares = None
    for a in range(ratio):
        term = own(a).astype(F32)
        term = jnp.sum(term * term, axis=1, keepdims=True)
        squares = term if squares is None else squares + term
    ssq2[j] = jnp.broadcast_to(squares, (rows, 128))
    for s in range(1, tp):
        start(remote(ssq2.at[j], ssq2.at[j], ts_sem.at[s], tr_sem.at[j], i, lax.rem(j + s, tp)))
    x = jnp.concatenate(
        [
            (
                rall[a].reshape(kv * rows, width).astype(F32)
                * mg_ref[:, a * width : (a + 1) * width].astype(F32)
            ).astype(BF16)
            for a in range(ratio)
        ],
        axis=1,
    )

    half = vu.shape[1] // 2
    chunks = usend.shape[0]
    piece = half // chunks
    core, across = lax.rem(j, 2), j // 2
    other = 1 - core
    partner = across * 2 + other

    def columns_of(h, c):
        return pl.ds(pl.multiple_of(h * half + c * piece, 128), piece)

    def give(c):
        usend[c] = dot(x, vu[:, columns_of(other, c)]).astype(BF16)
        start(remote(usend.at[c], urecv.at[c], us_sem.at[c], ur_sem.at[c], i, partner))

    give(0)
    for c in range(chunks):
        if c + 1 < chunks:
            give(c + 1)
        mine = dot(x, vu[:, columns_of(core, c)])
        remote(urecv.at[c], urecv.at[c], us_sem.at[c], ur_sem.at[c], i, partner).wait_recv()
        xsend[c] = (mine + urecv[c].astype(F32)).astype(BF16)
        for s in range(1, tp // 2):
            to = lax.rem(across + s, tp // 2)
            start(
                remote(
                    xsend.at[c], xrecv.at[across, c], xs_sem.at[s, c], xr_sem.at[across, c],
                    i, to * 2 + core,
                )
            )
    loads[7].wait()
    down = None
    for c in range(chunks):
        total = xsend[c].astype(F32)
        for s in range(1, tp // 2):
            at = lax.rem(across + s, tp // 2)
            slot_ref = xrecv.at[at, c]
            remote(
                slot_ref, slot_ref, xs_sem.at[0, c], xr_sem.at[at, c], i, at * 2 + core
            ).wait_recv()
            total = total + xrecv[at, c].astype(F32)
        act[core, c] = jnp.square(jnp.maximum(total, 0.0)).astype(BF16)
        start(
            remote(act.at[core, c], act.at[core, c], cs_sem.at[c], cr_sem.at[core, c], i, partner)
        )
        term = dot(act[core, c], vdn[columns_of(core, c), :])
        down = term if down is None else down + term
        arrive = act.at[other, c]
        remote(arrive, arrive, cs_sem.at[c], cr_sem.at[other, c], i, partner).wait_recv()
        down = down + dot(act[other, c], vdn[columns_of(other, c), :])
    dsend[...] = down.astype(BF16).reshape(dsend.shape)
    everyone(lambda k: dsend.at[k], drecv, ds_sem, dr_sem)

    for s in range(1, tp):
        k = lax.rem(j + s, tp)
        remote(ssq2.at[k], ssq2.at[k], ts_sem.at[0], tr_sem.at[k], i, k).wait_recv()
    squares = ssq2[0]
    for s in range(1, tp):
        squares = squares + ssq2[s]
    scale2 = lax.rsqrt(squares[:, :1] / (columns * tp) + epsilon)
    acc = dsend[i].astype(F32)
    for s in range(1, kv):
        k = arrived(drecv, ds_sem, dr_sem, s)
        acc = acc + drecv[k].astype(F32)
    acc = (acc * (scale2 * scale2)).astype(BF16).astype(F32)
    for a in range(ratio):
        at = slice(a * width, (a + 1) * width)
        out_ref[:, at] = (own(a).astype(F32) + acc[:, at]).astype(BF16)
    for copy, condition in sent:
        if condition is None:
            copy.wait_send()
        else:
            pl.when(condition)(copy.wait_send)


def layer(
    kv, tp, hidden_rows, carried, norm_gain, weights, decay_bias, head_gain, w_out, mlp_gain,
    w_up, w_down,
):
    rows, columns = hidden_rows.shape
    width = w_out.shape[1]
    ratio = kv // tp
    ny = inner_size(kv)
    nz = kv // ny
    cw = weights[0].shape[1]
    wide = weights[3].shape[1]
    pieces = sum(w.shape[1] for w in weights) // cw
    half = w_up.shape[1] // 2
    everything = kv * rows
    chunks = max(1, min(CHUNKS, half // 128))
    limit = VMEM_BYTES - 4 * carried.size - 128 * 1024
    vmem = pl.BlockSpec(memory_space=pltpu.VMEM)
    hbm = pl.BlockSpec(memory_space=pltpu.HBM)
    dma = pltpu.SemaphoreType.DMA
    wq, wk, wd_, wv, wg = weights
    return pl.pallas_call(
        functools.partial(layer_kernel, kv, tp),
        out_shape=[
            jax.ShapeDtypeStruct((rows, columns), BF16),
            pltpu.VMEM(carried.shape, F32),
        ],
        in_specs=[vmem] * 5 + [hbm] * 9,
        out_specs=[vmem, vmem],
        scratch_shapes=[
            pltpu.VMEM(w.shape, BF16) for w in (wq, wk, wd_, wv, wg, w_out, w_up, w_down)
        ]
        + [
            pltpu.VMEM((kv, rows, width), BF16),
            pltpu.VMEM((pieces, ny, nz, rows, cw), BF16),
            pltpu.VMEM((pieces, ny, nz, rows, cw), BF16),
            pltpu.VMEM((pieces, nz, rows, cw), BF16),
            pltpu.VMEM((pieces, nz, rows, cw), BF16),
            pltpu.VMEM((tp, rows, 128), F32),
            pltpu.VMEM((rows, cw), F32),
            pltpu.VMEM((rows, cw), F32),
            pltpu.VMEM((rows, cw), F32),
            pltpu.VMEM((rows, wide), F32),
            pltpu.VMEM((rows, wide), F32),
            pltpu.VMEM((rows, wide), BF16),
            pltpu.VMEM((kv, rows, wide), BF16),
            pltpu.VMEM((tp, ratio * rows, width), BF16),
            pltpu.VMEM((tp, ratio * rows, width), BF16),
            pltpu.VMEM((ratio * rows, width), BF16),
            pltpu.VMEM((ratio, tp, ratio * rows, width), BF16),
            pltpu.VMEM((chunks, everything, half // chunks), BF16),
            pltpu.VMEM((chunks, everything, half // chunks), BF16),
            pltpu.VMEM((chunks, everything, half // chunks), BF16),
            pltpu.VMEM((tp // 2, chunks, everything, half // chunks), BF16),
            pltpu.VMEM((2, chunks, everything, half // chunks), BF16),
            pltpu.VMEM((kv, rows, columns), BF16),
            pltpu.VMEM((kv, rows, columns), BF16),
            pltpu.VMEM((tp, rows, 128), F32),
            dma((8,)),
            dma,
            dma((kv,)),
            dma((kv,)),
            dma((tp,)),
            dma((tp,)),
            dma((pieces, ny)),
            dma((pieces, ny)),
            dma((pieces, nz)),
            dma((pieces, nz)),
            dma((kv,)),
            dma((kv,)),
            dma((tp,)),
            dma((tp,)),
            dma((kv,)),
            dma((ratio, tp)),
            dma((tp,)),
            dma((tp,)),
            dma((chunks,)),
            dma((chunks,)),
            dma((tp // 2, chunks)),
            dma((tp // 2, chunks)),
            dma((chunks,)),
            dma((2, chunks)),
            dma((kv,)),
            dma((kv,)),
        ],
        compiler_params=pltpu.CompilerParams(
            has_side_effects=True, collective_id=0, vmem_limit_bytes=limit
        ),
        name="layer",
    )(
        hidden_rows, norm_gain.reshape(1, -1), decay_bias.reshape(1, -1),
        head_gain.reshape(1, -1), mlp_gain.reshape(1, -1), wq, wk, wd_, wv, wg, carried,
        w_out, w_up, w_down,
    )


def body(
    kv,
    tp,
    hidden_rows,
    carried_state,
    norm_gain,
    w_query,
    w_key,
    w_decay,
    w_value,
    w_gate,
    decay_bias,
    head_gain,
    w_out,
    mlp_gain,
    w_up,
    w_down,
):
    updated_rows, new_state = layer(
        kv, tp, hidden_rows, carried_state, norm_gain,
        (w_query, w_key, w_decay, w_value, w_gate), decay_bias, head_gain, w_out, mlp_gain,
        w_up, w_down,
    )
    return (updated_rows, new_state)


def solution(mesh):
    return jax.shard_map(
        functools.partial(body, mesh.shape["kv"], mesh.shape["tp"]),
        mesh=mesh,
        in_specs=(
            P("kv", "tp"),
            P("kv", "tp"),
            P(),
            P("kv", "tp"),
            P("kv", "tp"),
            P("kv", "tp"),
            P("kv", "tp"),
            P("kv", "tp"),
            P("tp"),
            P(),
            P("tp", "kv"),
            P("tp"),
            P("tp", "kv"),
            P("kv", "tp"),
        ),
        out_specs=(P("kv", "tp"), P("kv", "tp")),
        check_vma=False,
    )
```

time: 95.1 us -> 78.2 us (0.82)
  Pallas kernels: 89.3 us -> 69.4 us
  local copies, waits for them, and re-layouts: 4.51 us -> 7.81 us
    pallas_call x3 -> x1, Pallas kernels: 89.3 us -> 69.4 us  [layer(): pl.pallas_call(functools.partial(layer_kernel, kv, tp), out_shape=[jax.Sh...]
    unnamed x3 -> x4, local copies, waits for them, and re-layouts: 1.38 us -> 4.02 us
where the time goes in v1:
time: 78.2 us; the launch traced here: 77.8 us
  Pallas kernels  69.4 us (89%)
  local copies, waits for them, and re-layouts  7.81 us (10%)
    pallas_call x1, Pallas kernels, layer(): pl.pallas_call(functools.partial(layer_kernel, kv, tp), out_shape=[jax.Sh...  69.4 us
    unnamed x4, local copies, waits for them, and re-layouts  4.02 us

profile of v1, /device:TPU:0, one launch (start us, length us, event | category | flops | bytes accessed | tf_op | source)
XLA Modules:
  0.0 77.8 jit_solution(5863650228643699387)
XLA Ops:
  0.6 1.2 %reshape.18.hg_ref = bf16[1,256]{1,0:T(2,128)(2,1)} reshape(bf16[256]{0:T(256)(128)(2,1)} %param.23) | data formatting | bytes 1024 | tf_op jit(solution)/shard_map/reshape | solution.py:470
  1.8 1.3 %reshape.19.mg_ref = bf16[1,1024]{1,0:T(2,128)(2,1)} reshape(bf16[1024]{0:T(1024)(128)(2,1)} %param.25) | data formatting | bytes 4096 | tf_op jit(solution)/shard_map/reshape | solution.py:470
  3.1 1.3 %reshape.16.ng_ref = bf16[1,4096]{1,0:T(2,128)(2,1)} reshape(bf16[4096]{0:T(1024)(128)(2,1)} %param.16) | data formatting | bytes 16384 | tf_op jit(solution)/shard_map/reshape | solution.py:469
  4.4 69.4 %layer.1 = (bf16[16,1024]{1,0:T(8,128)(2,1)}, f32[16,131072]{1,0:T(8,128)S(1)}) custom-call(bf16[16,1024]{1,0:T(8,128)(2,1)} %h_ref.1, bf16[1,4096]{1,0:T(2,128)(2,1)} %reshape.16.ng_ref, f32[1,512]{1,0:T(1,128)} %bitcast.1, bf16[1,256]{1,0:T(2,128)(2,1)} %reshape.18.hg_ref, bf16[1,1024]{1,0:T(2,128)(2,1)} %reshape.19.mg_ref, bf16[512,512]{1,0:T(8,128)(2,1)} %wq.1, ...), custom_call_target="tpu_custom_call" | custom-call | tf_op jit(solution)/shard_map/layer/pallas_call | solution.py:400
  73.8 0.0 copy-start
  73.8 3.4 %copy.18 = f32[16,131072]{1,0:T(8,128)} copy(f32[16,131072]{1,0:T(8,128)S(1)} %get-tuple-element.3) | data formatting | bytes 16777216
  77.2 0.0 copy-done
  77.2 0.6 copy.19
Async XLA Ops:
  73.8 3.4 %copy-start = (bf16[16,1024]{1,0:T(8,128)(2,1)S(1)}, bf16[16,1024]{1,0:T(8,128)(2,1)}, u32[]{:S(2)}) copy-start(bf16[16,1024]{1,0:T(8,128)(2,1)} %get-tuple-element.6) | copy-start | bytes 98308

commit v2 on v1

--- a/solution.py
+++ b/solution.py
@@ -16,7 +16,8 @@
 F32 = jnp.float32
 BF16 = jnp.bfloat16
 MESH = pl.DeviceIdType.MESH
-CHUNKS = 4
+CHUNKS = 2
+STORES = 8
 VMEM_BYTES = 67043328
 
 
@@ -44,12 +45,13 @@
 
 def layer_kernel(
     kv, tp,
-    h_ref, ng_ref, bias_ref, hg_ref, mg_ref, wq, wk, wd_, wv, wg, old, wo, wu, wdn,
+    h_in, ng_in, bias_in, hg_in, mg_in, wq, wk, wd_, wv, wg, old, wo, wu, wdn,
     out_ref, st_ref,
+    h_ref, ng_ref, bias_ref, hg_ref, mg_ref, gains,
     vq, vk, vd_, vv, vg, vo, vu, vdn,
     xbuf, psnd, prcv, zsnd, zrcv, ssq, query, key, decay, value, head,
     mixed, mall, asend, arecv, rpart, rall, usend, urecv, xsend, xrecv, act, dsend, drecv, ssq2,
-    wsem, stsem, hs_sem, hr_sem, ss_sem, sr_sem, ps_sem, pr_sem, qs_sem, qr_sem,
+    insem, wsem, stsem, hs_sem, hr_sem, fs_sem, ss_sem, sr_sem, ps_sem, pr_sem, qs_sem, qr_sem,
     ms_sem, mr_sem, as_sem, ar_sem, rs_sem, rr_sem, ts_sem, tr_sem,
     us_sem, ur_sem, xs_sem, xr_sem, cs_sem, cr_sem, ds_sem, dr_sem,
 ):
@@ -74,6 +76,14 @@
         pl.when(condition)(copy.start)
         sent.append((copy, condition))
 
+    inputs = [
+        pltpu.make_async_copy(src, dst, insem.at[n])
+        for n, (src, dst) in enumerate(
+            ((h_in, h_ref), (ng_in, ng_ref), (bias_in, bias_ref), (hg_in, hg_ref), (mg_in, mg_ref))
+        )
+    ]
+    for copy in inputs:
+        copy.start()
     barrier = pltpu.get_barrier_semaphore()
 
     def greet(a, b):
@@ -111,38 +121,48 @@
     for load in loads[5:]:
         load.start()
 
+    for copy in inputs:
+        copy.wait()
     hidden = h_ref[...].astype(F32)
     ssq[j] = jnp.broadcast_to(jnp.sum(hidden * hidden, axis=1, keepdims=True), (rows, 128))
     itself = jnp.where(owner == j, 1, 0)
     pl.semaphore_wait(barrier, 2 * (kv - itself) + (kv - 1) + (tp - 1))
 
+    side = lax.rem(i, 2)
     for a in range(ratio):
-        for s in range(tp):
-            k, t = j * ratio + a, lax.rem(j + s, tp)
-            copy = remote(
-                h_ref.at[:, pl.ds(a * width, width)], xbuf.at[i],
-                hs_sem.at[a * tp + s], hr_sem.at[i], k, t,
-            )
+        k = j * ratio + a
+        src = h_ref.at[:, pl.ds(a * width, width)]
+        for s in range(tp // 2):
+            t = lax.rem(j // 2 + s, tp // 2) * 2 + side
+            copy = remote(src, xbuf.at[i], hs_sem.at[a * (tp // 2) + s], hr_sem.at[i], k, t)
             if s:
                 start(copy)
             else:
-                start_if(k != i, copy)
-
-                @pl.when(k == i)
+                start_if(jnp.logical_or(k != i, t != j), copy)
+
+                @pl.when(jnp.logical_and(k == i, t == j))
                 def _():
                     xbuf[i] = h_ref[:, a * width : (a + 1) * width]
 
     for s in range(1, tp):
         start(remote(ssq.at[j], ssq.at[j], ss_sem.at[s], sr_sem.at[j], i, lax.rem(j + s, tp)))
 
-    gain = ng_ref[:, pl.ds(pl.multiple_of(i * width, 128), width)].astype(F32)
-    for s in range(kv):
-        k = lax.rem(i + s, kv)
+    gains[...] = ng_ref[...].astype(F32).reshape(1, kv * width)
+    gain = gains[:, pl.ds(pl.multiple_of(i * width, 128), width)]
+    core = lax.rem(j, 2)
+    partner = j + 1 - 2 * core
+    even = i - lax.rem(i, 2)
+    for s in range(kv // 2):
+        k = lax.rem(even + 2 * s, kv) + core
         arrive = remote(xbuf.at[k], xbuf.at[k], hs_sem.at[0], hr_sem.at[k], k, owner)
         if s:
             arrive.wait_recv()
         else:
-            pl.when(owner != j)(arrive.wait_recv)
+            pl.when(jnp.logical_or(owner != j, k != i))(arrive.wait_recv)
+        start(remote(xbuf.at[k], xbuf.at[k], fs_sem.at[s], hr_sem.at[k], i, partner))
+    for s in range(kv // 2):
+        k = lax.rem(even + 2 * s, kv) + 1 - core
+        remote(xbuf.at[k], xbuf.at[k], fs_sem.at[0], hr_sem.at[k], i, partner).wait_recv()
     x = (xbuf[...].reshape(kv * rows, width).astype(F32) * gain).astype(BF16)
 
     pieces = []
@@ -205,24 +225,35 @@
     decay[...] = jnp.exp(log_decay / decay_normalizer)
     key[...] = reduced(1)
     query[...] = reduced(2) * DK ** (-0.5)
+    load_state.wait()
+
+    def head_slices(h):
+        narrow = pl.ds(pl.multiple_of(h * DK, DK), DK)
+        wide = pl.ds(pl.multiple_of(h * DV, DV), DV)
+        return narrow, wide
+
+    def state_slice(h, c):
+        return pl.ds(pl.multiple_of(h * (DK * DV) + c * DV, DV), DV)
+
+    @pl.loop(0, heads)
+    def _(h):
+        narrow, wide = head_slices(h)
+        q = query[:, narrow] * decay[:, narrow]
+        acc = jnp.zeros((rows, DV), F32)
+        for c in range(DK):
+            acc = acc + q[:, c : c + 1] * st_ref[:, state_slice(h, c)]
+        head[:, wide] = acc
+
     for c in range(3, 5):
         value[:, (c - 3) * cw : (c - 2) * cw] = reduced(c)
-    load_state.wait()
-
-    @pl.loop(0, heads)
-    def _(h):
-        narrow = pl.ds(pl.multiple_of(h * DK, DK), DK)
-        wide = pl.ds(pl.multiple_of(h * DV, DV), DV)
-        q, k, d = query[:, narrow], key[:, narrow], decay[:, narrow]
-        v = value[:, wide]
-        acc = jnp.zeros((rows, DV), F32)
-        for c in range(DK):
-            at = pl.ds(pl.multiple_of(h * (DK * DV) + c * DV, DV), DV)
-            new = d[:, c : c + 1] * st_ref[:, at] + k[:, c : c + 1] * v
-            st_ref[:, at] = new
-            acc = acc + q[:, c : c + 1] * new
+    head_gain = hg_ref[...].astype(F32).reshape(1, DV)
+    for h in range(heads):
+        at = slice(h * DK, (h + 1) * DK)
+        weight = jnp.sum(query[:, at] * key[:, at], axis=1, keepdims=True)
+        at = slice(h * DV, (h + 1) * DV)
+        acc = head[:, at] + weight * value[:, at]
         acc = acc * lax.rsqrt(jnp.mean(acc * acc, axis=1, keepdims=True) + epsilon)
-        head[:, wide] = acc * hg_ref[...].astype(F32)
+        head[:, at] = acc * head_gain
 
     for c in range(5, 7):
         at = slice((c - 5) * cw, (c - 4) * cw)
@@ -240,6 +271,7 @@
 
     everyone(lambda k: mixed, mall, ms_sem, mr_sem)
     mall[i] = mixed[...]
+
     loads[5].wait()
     for s in range(1, kv):
         arrived(mall, ms_sem, mr_sem, s)
@@ -254,36 +286,132 @@
         remote(arecv.at[t], arecv.at[t], as_sem.at[0], ar_sem.at[t], i, t).wait_recv()
         attn = attn + arecv[t].astype(F32)
     mine = xbuf[pl.ds(j * ratio, ratio)].reshape(ratio * rows, width).astype(F32)
-    rpart[...] = (mine + attn.astype(BF16).astype(F32)).astype(BF16)
+    res = (mine + attn.astype(BF16).astype(F32)).astype(BF16)
+    for m in range(ratio):
+        rpart[m % 2, m // 2 * rows : (m // 2 + 1) * rows] = res[m * rows : (m + 1) * rows]
 
     slot = lax.rem(i, ratio)
-    for s in range(kv):
-        k = lax.rem(i + s, kv)
-        copy = remote(rpart, rall.at[slot, j], rs_sem.at[s], rr_sem.at[slot, j], k, owner)
-        if s:
-            start(copy)
-        else:
-            start_if(owner != j, copy)
+    for p in range(2):
+        for s in range(kv):
+            k = lax.rem(i + s, kv)
+            copy = remote(
+                rpart.at[p], rall.at[slot, p, j], rs_sem.at[p, s], rr_sem.at[slot, p, j], k, owner
+            )
+            if s:
+                start(copy)
+            else:
+                start_if(owner != j, copy)
 
     @pl.when(owner == j)
     def _():
-        rall[slot, j] = rpart[...]
+        for p in range(2):
+            rall[slot, p, j] = rpart[p]
+
+    @pl.loop(0, heads)
+    def _(h):
+        narrow, wide = head_slices(h)
+        k, d = key[:, narrow], decay[:, narrow]
+        v = value[:, wide]
+        for c in range(DK):
+            at = state_slice(h, c)
+            st_ref[:, at] = d[:, c : c + 1] * st_ref[:, at] + k[:, c : c + 1] * v
 
     loads[6].wait()
-    for a in range(ratio):
-        k = j * ratio + a
-        for s in range(tp):
-            t = lax.rem(j + s, tp)
-            at = rall.at[a, t]
-            arrive = remote(at, at, rs_sem.at[0], rr_sem.at[a, t], k, t)
+    mlp_gain = mg_ref[...].astype(F32).reshape(1, columns)
+    tokens = kv // 2 * rows
+
+    def gathered(p):
+        for a in range(ratio):
+            k = j * ratio + a
+            for s in range(tp):
+                t = lax.rem(j + s, tp)
+                at = rall.at[a, p, t]
+                arrive = remote(at, at, rs_sem.at[p, 0], rr_sem.at[a, p, t], k, t)
+                if s:
+                    arrive.wait_recv()
+                else:
+                    pl.when(k != i)(arrive.wait_recv)
+        return jnp.concatenate(
+            [
+                (
+                    rall[a, p].reshape(tokens, width).astype(F32)
+                    * mlp_gain[:, a * width : (a + 1) * width]
+                ).astype(BF16)
+                for a in range(ratio)
+            ],
+            axis=1,
+        )
+
+    def own(a):
+        low = pl.multiple_of(slot // 2 * rows, rows)
+        return rall[a, lax.rem(slot, 2), owner, pl.ds(low, rows), :]
+
+    half = vu.shape[1] // 2
+    chunks = usend.shape[1]
+    piece = half // chunks
+    across = j // 2
+    other = 1 - core
+
+    def columns_of(h, c):
+        return pl.ds(pl.multiple_of(h * half + c * piece, 128), piece)
+
+    def up(p, x):
+        def give(c):
+            usend[p, c] = dot(x, vu[:, columns_of(other, c)]).astype(BF16)
+            start(
+                remote(
+                    usend.at[p, c], urecv.at[p, c], us_sem.at[p, c], ur_sem.at[p, c], i, partner
+                )
+            )
+
+        give(0)
+        for c in range(chunks):
+            if c + 1 < chunks:
+                give(c + 1)
+            mine = dot(x, vu[:, columns_of(core, c)])
+            at = urecv.at[p, c]
+            remote(at, at, us_sem.at[p, c], ur_sem.at[p, c], i, partner).wait_recv()
+            xsend[p, c] = (mine + urecv[p, c].astype(F32)).astype(BF16)
+            for s in range(1, tp // 2):
+                to = lax.rem(across + s, tp // 2)
+                start(
+                    remote(
+                        xsend.at[p, c], xrecv.at[p, across, c],
+                        xs_sem.at[p, s, c], xr_sem.at[p, across, c], i, to * 2 + core,
+                    )
+                )
+
+    def down(p):
+        acc = None
+        for c in range(chunks):
+            total = xsend[p, c].astype(F32)
+            for s in range(1, tp // 2):
+                at = lax.rem(across + s, tp // 2)
+                ref = xrecv.at[p, at, c]
+                remote(
+                    ref, ref, xs_sem.at[p, 0, c], xr_sem.at[p, at, c], i, at * 2 + core
+                ).wait_recv()
+                total = total + xrecv[p, at, c].astype(F32)
+            act[p, core, c] = jnp.square(jnp.maximum(total, 0.0)).astype(BF16)
+            ref = act.at[p, core, c]
+            start(remote(ref, ref, cs_sem.at[p, c], cr_sem.at[p, core, c], i, partner))
+            term = dot(act[p, core, c], vdn[columns_of(core, c), :])
+            acc = term if acc is None else acc + term
+            ref = act.at[p, other, c]
+            remote(ref, ref, cs_sem.at[p, c], cr_sem.at[p, other, c], i, partner).wait_recv()
+            acc = acc + dot(act[p, other, c], vdn[columns_of(other, c), :])
+        dsend[p] = acc.astype(BF16).reshape(dsend.shape[1:])
+        for s in range(kv // 2):
+            kk = lax.rem(i // 2 + s, kv // 2)
+            k = 2 * kk + p
+            copy = remote(dsend.at[p, kk], drecv.at[i], ds_sem.at[p, s], dr_sem.at[i], k, j)
             if s:
-                arrive.wait_recv()
+                start(copy)
             else:
-                pl.when(k != i)(arrive.wait_recv)
-
-    def own(a):
-        return rall[a, owner, pl.ds(pl.multiple_of(slot * rows, rows), rows), :]
-
+                start_if(k != i, copy)
+
+    up(0, gathered(0))
+    x1 = gathered(1)
     squares = None
     for a in range(ratio):
         term = own(a).astype(F32)
@@ -292,68 +420,10 @@
     ssq2[j] = jnp.broadcast_to(squares, (rows, 128))
     for s in range(1, tp):
         start(remote(ssq2.at[j], ssq2.at[j], ts_sem.at[s], tr_sem.at[j], i, lax.rem(j + s, tp)))
-    x = jnp.concatenate(
-        [
-            (
-                rall[a].reshape(kv * rows, width).astype(F32)
-                * mg_ref[:, a * width : (a + 1) * width].astype(F32)
-            ).astype(BF16)
-            for a in range(ratio)
-        ],
-        axis=1,
-    )
-
-    half = vu.shape[1] // 2
-    chunks = usend.shape[0]
-    piece = half // chunks
-    core, across = lax.rem(j, 2), j // 2
-    other = 1 - core
-    partner = across * 2 + other
-
-    def columns_of(h, c):
-        return pl.ds(pl.multiple_of(h * half + c * piece, 128), piece)
-
-    def give(c):
-        usend[c] = dot(x, vu[:, columns_of(other, c)]).astype(BF16)
-        start(remote(usend.at[c], urecv.at[c], us_sem.at[c], ur_sem.at[c], i, partner))
-
-    give(0)
-    for c in range(chunks):
-        if c + 1 < chunks:
-            give(c + 1)
-        mine = dot(x, vu[:, columns_of(core, c)])
-        remote(urecv.at[c], urecv.at[c], us_sem.at[c], ur_sem.at[c], i, partner).wait_recv()
-        xsend[c] = (mine + urecv[c].astype(F32)).astype(BF16)
-        for s in range(1, tp // 2):
-            to = lax.rem(across + s, tp // 2)
-            start(
-                remote(
-                    xsend.at[c], xrecv.at[across, c], xs_sem.at[s, c], xr_sem.at[across, c],
-                    i, to * 2 + core,
-                )
-            )
+    up(1, x1)
     loads[7].wait()
-    down = None
-    for c in range(chunks):
-        total = xsend[c].astype(F32)
-        for s in range(1, tp // 2):
-            at = lax.rem(across + s, tp // 2)
-            slot_ref = xrecv.at[at, c]
-            remote(
-                slot_ref, slot_ref, xs_sem.at[0, c], xr_sem.at[at, c], i, at * 2 + core
-            ).wait_recv()
-            total = total + xrecv[at, c].astype(F32)
-        act[core, c] = jnp.square(jnp.maximum(total, 0.0)).astype(BF16)
-        start(
-            remote(act.at[core, c], act.at[core, c], cs_sem.at[c], cr_sem.at[core, c], i, partner)
-        )
-        term = dot(act[core, c], vdn[columns_of(core, c), :])
-        down = term if down is None else down + term
-        arrive = act.at[other, c]
-        remote(arrive, arrive, cs_sem.at[c], cr_sem.at[other, c], i, partner).wait_recv()
-        down = down + dot(act[other, c], vdn[columns_of(other, c), :])
-    dsend[...] = down.astype(BF16).reshape(dsend.shape)
-    everyone(lambda k: dsend.at[k], drecv, ds_sem, dr_sem)
+    down(0)
+    down(1)
 
     for s in range(1, tp):
         k = lax.rem(j + s, tp)
@@ -362,9 +432,9 @@
     for s in range(1, tp):
         squares = squares + ssq2[s]
     scale2 = lax.rsqrt(squares[:, :1] / (columns * tp) + epsilon)
-    acc = dsend[i].astype(F32)
+    acc = dsend[lax.rem(i, 2), i // 2].astype(F32)
     for s in range(1, kv):
-        k = arrived(drecv, ds_sem, dr_sem, s)
+        k = arrived(drecv, ds_sem.at[0], dr_sem, s)
         acc = acc + drecv[k].astype(F32)
     acc = (acc * (scale2 * scale2)).astype(BF16).astype(F32)
     for a in range(ratio):
@@ -390,22 +460,29 @@
     wide = weights[3].shape[1]
     pieces = sum(w.shape[1] for w in weights) // cw
     half = w_up.shape[1] // 2
-    everything = kv * rows
+    tokens = kv // 2 * rows
     chunks = max(1, min(CHUNKS, half // 128))
+    piece = half // chunks
     limit = VMEM_BYTES - 4 * carried.size - 128 * 1024
     vmem = pl.BlockSpec(memory_space=pltpu.VMEM)
     hbm = pl.BlockSpec(memory_space=pltpu.HBM)
     dma = pltpu.SemaphoreType.DMA
     wq, wk, wd_, wv, wg = weights
+    bias = decay_bias.reshape(1, -1)
     return pl.pallas_call(
         functools.partial(layer_kernel, kv, tp),
         out_shape=[
-            jax.ShapeDtypeStruct((rows, columns), BF16),
+            pltpu.VMEM((rows, columns), BF16),
             pltpu.VMEM(carried.shape, F32),
         ],
-        in_specs=[vmem] * 5 + [hbm] * 9,
+        in_specs=[hbm] * 14,
         out_specs=[vmem, vmem],
         scratch_shapes=[
+            pltpu.VMEM(a.shape, a.dtype)
+            for a in (hidden_rows, norm_gain, bias, head_gain, mlp_gain)
+        ]
+        + [pltpu.VMEM((1, norm_gain.shape[0]), F32)]
+        + [
             pltpu.VMEM(w.shape, BF16) for w in (wq, wk, wd_, wv, wg, w_out, w_up, w_down)
         ]
         + [
@@ -424,18 +501,20 @@
             pltpu.VMEM((kv, rows, wide), BF16),
             pltpu.VMEM((tp, ratio * rows, width), BF16),
             pltpu.VMEM((tp, ratio * rows, width), BF16),
-            pltpu.VMEM((ratio * rows, width), BF16),
-            pltpu.VMEM((ratio, tp, ratio * rows, width), BF16),
-            pltpu.VMEM((chunks, everything, half // chunks), BF16),
-            pltpu.VMEM((chunks, everything, half // chunks), BF16),
-            pltpu.VMEM((chunks, everything, half // chunks), BF16),
-            pltpu.VMEM((tp // 2, chunks, everything, half // chunks), BF16),
-            pltpu.VMEM((2, chunks, everything, half // chunks), BF16),
-            pltpu.VMEM((kv, rows, columns), BF16),
+            pltpu.VMEM((2, ratio // 2 * rows, width), BF16),
+            pltpu.VMEM((ratio, 2, tp, ratio // 2 * rows, width), BF16),
+            pltpu.VMEM((2, chunks, tokens, piece), BF16),
+            pltpu.VMEM((2, chunks, tokens, piece), BF16),
+            pltpu.VMEM((2, chunks, tokens, piece), BF16),
+            pltpu.VMEM((2, tp // 2, chunks, tokens, piece), BF16),
+            pltpu.VMEM((2, 2, chunks, tokens, piece), BF16),
+            pltpu.VMEM((2, kv // 2, rows, columns), BF16),
             pltpu.VMEM((kv, rows, columns), BF16),
             pltpu.VMEM((tp, rows, 128), F32),
+            dma((5,)),
             dma((8,)),
             dma,
+            dma((kv,)),
             dma((kv,)),
             dma((kv,)),
             dma((tp,)),
@@ -448,17 +527,17 @@
             dma((kv,)),
             dma((tp,)),
             dma((tp,)),
-            dma((kv,)),
-            dma((ratio, tp)),
+            dma((2, kv)),
+            dma((ratio, 2, tp)),
             dma((tp,)),
             dma((tp,)),
-            dma((chunks,)),
-            dma((chunks,)),
-            dma((tp // 2, chunks)),
-            dma((tp // 2, chunks)),
-            dma((chunks,)),
             dma((2, chunks)),
-            dma((kv,)),
+            dma((2, chunks)),
+            dma((2, tp // 2, chunks)),
+            dma((2, tp // 2, chunks)),
+            dma((2, chunks)),
+            dma((2, 2, chunks)),
+            dma((2, kv // 2)),
             dma((kv,)),
         ],
         compiler_params=pltpu.CompilerParams(
@@ -466,10 +545,39 @@
         ),
         name="layer",
     )(
-        hidden_rows, norm_gain.reshape(1, -1), decay_bias.reshape(1, -1),
-        head_gain.reshape(1, -1), mlp_gain.reshape(1, -1), wq, wk, wd_, wv, wg, carried,
+        hidden_rows, norm_gain, bias, head_gain, mlp_gain, wq, wk, wd_, wv, wg, carried,
         w_out, w_up, w_down,
     )
+
+
+def store_kernel(parts, new_in, rows_in, new_out, rows_out, sems):
+    size = new_in.shape[1] // parts
+    copies = [pltpu.make_async_copy(rows_in, rows_out, sems.at[parts])]
+    for n in range(parts):
+        at = pl.ds(n * size, size)
+        copies.append(pltpu.make_async_copy(new_in.at[:, at], new_out.at[:, at], sems.at[n]))
+    for copy in copies:
+        copy.start()
+    for copy in copies:
+        copy.wait()
+
+
+def store(updated_rows, new_state):
+    parts = STORES
+    vmem = pl.BlockSpec(memory_space=pltpu.VMEM)
+    hbm = pl.BlockSpec(memory_space=pltpu.HBM)
+    return pl.pallas_call(
+        functools.partial(store_kernel, parts),
+        out_shape=[
+            jax.ShapeDtypeStruct(new_state.shape, new_state.dtype),
+            jax.ShapeDtypeStruct(updated_rows.shape, updated_rows.dtype),
+        ],
+        in_specs=[vmem, vmem],
+        out_specs=[hbm, hbm],
+        scratch_shapes=[pltpu.SemaphoreType.DMA((parts + 1,))],
+        compiler_params=pltpu.CompilerParams(vmem_limit_bytes=1024 * 1024),
+        name="store",
+    )(new_state, updated_rows)
 
 
 def body(
@@ -495,6 +603,7 @@
         (w_query, w_key, w_decay, w_value, w_gate), decay_bias, head_gain, w_out, mlp_gain,
         w_up, w_down,
     )
+    new_state, updated_rows = store(updated_rows, new_state)
     return (updated_rows, new_state)
 
 

time: 78.2 us -> 65 us (0.83)
  local copies, waits for them, and re-layouts: 7.81 us -> 0 us
  Pallas kernels: 69.4 us -> 63.2 us
    pallas_call x1 -> x2, Pallas kernels: 69.4 us -> 63.2 us  [the longest x1 59.9 us: layer(): pl.pallas_call(functools.partial(layer_kernel, kv, tp), out_shape=[pltpu....]
    unnamed x4 -> x0, local copies, waits for them, and re-layouts: 4.02 us -> none
    reshape x3 -> x0, local copies, waits for them, and re-layouts: 3.79 us -> none  [the longest x1 1.31 us: layer(): norm_gain.reshape(1, -1)]
where the time goes in v2:
time: 65 us; the launch traced here: 63.9 us
  Pallas kernels  63.2 us (97%)
    pallas_call x1, Pallas kernels, layer(): pl.pallas_call(functools.partial(layer_kernel, kv, tp), out_shape=[pltpu....  59.9 us
    pallas_call x1, Pallas kernels, store(): pl.pallas_call(functools.partial(store_kernel, parts), out_shape=[jax.Sha...  3.39 us

profile of v2, /device:TPU:0, one launch (start us, length us, event | category | flops | bytes accessed | tf_op | source)
XLA Modules:
  0.0 63.9 jit_solution(17766789449449632607)
XLA Ops:
  0.6 59.9 %layer.1 = (bf16[16,1024]{1,0:T(8,128)(2,1)S(1)}, f32[16,131072]{1,0:T(8,128)S(1)}) custom-call(bf16[16,1024]{1,0:T(8,128)(2,1)} %h_in.1, bf16[4096]{0:T(1024)(128)(2,1)} %ng_in.1, f32[1,512]{1,0:T(1,128)} %bitcast.1, bf16[256]{0:T(256)(128)(2,1)} %hg_in.1, bf16[1024]{0:T(1024)(128)(2,1)} %mg_in.1, bf16[512,512]{1,0:T(8,128)(2,1)} %wq.1, ...), custom_call_target="tpu_custom_call" | custom-call | tf_op jit(solution)/shard_map/layer/pallas_call | solution.py:472
  60.5 3.4 %store.1 = (f32[16,131072]{1,0:T(8,128)}, bf16[16,1024]{1,0:T(8,128)(2,1)}) custom-call(f32[16,131072]{1,0:T(8,128)S(1)} %get-tuple-element.6.new_in, bf16[16,1024]{1,0:T(8,128)(2,1)S(1)} %get-tuple-element.7.rows_in), custom_call_target="tpu_custom_call" | custom-call | tf_op jit(solution)/shard_map/store/pallas_call | solution.py:569

commit v3 on v2

v3 whole, which is shorter than its diff:
```python
import functools

import jax
import jax.numpy as jnp
from jax import lax
from jax.experimental import pallas as pl
from jax.experimental.pallas import tpu as pltpu
from jax.sharding import PartitionSpec as P

DK = 128
DV = 256

epsilon = 1e-06
decay_normalizer = 16.0

F32 = jnp.float32
BF16 = jnp.bfloat16
MESH = pl.DeviceIdType.MESH
CHUNKS = 2
SPLIT = 1
LATE = 1
ONES = 19
STORES = 8
VMEM_BYTES = 67043328


def remote(src, dst, send_sem, recv_sem, i, j):
    return pltpu.make_async_remote_copy(
        src_ref=src,
        dst_ref=dst,
        send_sem=send_sem,
        recv_sem=recv_sem,
        device_id={"kv": i, "tp": j},
        device_id_type=MESH,
    )


def dot(a, b):
    return jnp.dot(a, b, preferred_element_type=F32)


def inner_size(kv):
    size = 1
    while (size * 2) ** 2 <= kv:
        size = size * 2
    return size


def layer_kernel(
    kv, tp,
    h_in, ng_in, bias_in, hg_in, mg_in, wq, wk, wd_, wv, wg, old, wo, wu, wdn,
    out_ref, st_ref,
    h_ref, ng_ref, bias_ref, hg_ref, mg_ref, gains,
    vq, vk, vd_, vv, vg, vo, vu, vdn,
    xbuf, psnd, prcv, zsnd, zrcv, wsnd, wrcv, vsnd, vrcv, ssq, query, key, decay, value, head,
    mixed, mall, asend, arecv, rpart, rall, usend, urecv, xsend, xrecv, act, dsend, drecv, ssq2,
    insem, wsem, hr_sem, pr_sem, qr_sem, wr_sem, er_sem, mr_sem, ar_sem, rr_sem,
    ur_sem, xr_sem, cr_sem, dr_sem, one,
):
    i, j = lax.axis_index("kv"), lax.axis_index("tp")
    ny = inner_size(kv)
    nz = kv // ny
    z, y = i // ny, lax.rem(i, ny)
    ratio = kv // tp
    owner = i // ratio
    rows = h_ref.shape[0]
    eight = rows // 2
    columns = h_ref.shape[1]
    width = xbuf.shape[2]
    cw = vq.shape[1]
    pw = psnd.shape[4]
    heads = cw // DK
    core = lax.rem(j, 2)
    across = j // 2
    other = 1 - core
    partner = across * 2 + other
    (
        st_sem, hs_sem, fs_sem, fr_sem, ss_sem, sr_sem, ps_sem, qs_sem, ws_sem, es_sem,
        ms_sem, as_sem, rs_sem, ts_sem, tr_sem, us_sem, xs_sem, cs_sem, ds_sem,
    ) = [one.at[n] for n in range(ONES)]

    def take(ref, sem):
        remote(ref, ref, sem, sem, i, partner).wait_recv()

    def drain(ref, sem):
        remote(ref, ref, sem, sem, i, partner).wait_send()

    def send(src, dst, send_sem, recv_sem, a, b):
        remote(src, dst, send_sem, recv_sem, a, b).start()

    inputs = [
        pltpu.make_async_copy(src, dst, insem.at[n])
        for n, (src, dst) in enumerate(
            ((h_in, h_ref), (ng_in, ng_ref), (bias_in, bias_ref), (hg_in, hg_ref), (mg_in, mg_ref))
        )
    ]
    for copy in inputs:
        copy.start()
    barrier = pltpu.get_barrier_semaphore()

    def greet(a, b):
        pl.semaphore_signal(
            barrier, inc=1, device_id={"kv": a, "tp": b}, device_id_type=MESH
        )

    for s in range(kv):
        k = lax.rem(i + s, kv)
        if s:
            greet(k, owner)
            greet(k, j)
        else:
            pl.when(owner != j)(lambda: greet(i, owner))
    for a in range(ratio):
        for s in range(tp):
            k, t = j * ratio + a, lax.rem(j + s, tp)
            if s:
                greet(k, t)
            else:
                pl.when(k != i)(functools.partial(greet, k, t))
    for s in range(1, tp):
        greet(i, lax.rem(j + s, tp))

    loads = [
        pltpu.make_async_copy(w, v, wsem.at[n])
        for n, (w, v) in enumerate(
            ((wd_, vd_), (wk, vk), (wq, vq), (wv, vv), (wg, vg), (wo, vo), (wu, vu), (wdn, vdn))
        )
    ]
    load_state = pltpu.make_async_copy(old, st_ref, st_sem)
    for load in loads[:5]:
        load.start()
    load_state.start()
    for load in loads[5:]:
        load.start()

    for copy in inputs:
        copy.wait()
    hidden = h_ref[...].astype(F32)
    ssq[j] = jnp.broadcast_to(jnp.sum(hidden * hidden, axis=1, keepdims=True), (rows, 128))
    itself = jnp.where(owner == j, 1, 0)
    pl.semaphore_wait(barrier, 2 * (kv - itself) + (kv - 1) + (tp - 1))

    side = lax.rem(i, 2)
    for a in range(ratio):
        k = j * ratio + a
        for s in range(tp // 2):
            t = lax.rem(across + s, tp // 2) * 2 + side
            copy = remote(
                h_ref.at[:, pl.ds(a * width, width)], xbuf.at[i], hs_sem, hr_sem.at[i // 2], k, t
            )
            if s:
                copy.start()
            else:
                here = jnp.logical_and(k == i, t == j)
                pl.when(jnp.logical_not(here))(copy.start)

                @pl.when(here)
                def _():
                    xbuf[i] = h_ref[:, a * width : (a + 1) * width]

    for s in range(1, tp):
        send(ssq.at[j], ssq.at[j], ss_sem, sr_sem, i, lax.rem(j + s, tp))

    gains[...] = ng_ref[...].astype(F32).reshape(1, kv * width)
    gain = gains[:, pl.ds(pl.multiple_of(i * width, 128), width)]
    for s in range(kv // 2):
        m = lax.rem(i // 2 + s, kv // 2)
        k = 2 * m + core
        if s:
            take(xbuf.at[k], hr_sem.at[m])
        else:
            pl.when(jnp.logical_or(owner != j, k != i))(lambda: take(xbuf.at[k], hr_sem.at[m]))
        send(xbuf.at[k], xbuf.at[k], fs_sem, fr_sem, i, partner)
    take(xbuf.at[pl.ds(0, kv // 2)], fr_sem)
    x = (xbuf[...].reshape(kv * rows, width).astype(F32) * gain).astype(BF16)

    pieces = []
    for n, v in enumerate((vd_, vk, vq, vv, vg)):
        for low in range(0, v.shape[1], pw):
            pieces.append((n, v, low))
    late = len(pieces) - wsnd.shape[0]
    ready = set()

    def product(c):
        n, v, low = pieces[c]
        if n not in ready:
            loads[n].wait()
            ready.add(n)
        return dot(x, v[:, low : low + pw]).astype(BF16)

    def first_z(c):
        part, e = product(c), c - late
        for zz in range(nz):
            for yy in range(ny):
                at = (zz * ny + yy) * rows
                wsnd[e, zz, yy] = part[at : at + rows]
        for s in range(1, nz):
            zz = lax.rem(z + s, nz)
            send(wsnd.at[e, zz], wrcv.at[e, s - 1], ws_sem, wr_sem.at[e], zz * ny + y, j)

    def first_y(c):
        part = product(c)
        for zz in range(nz):
            for yy in range(ny):
                at = (zz * ny + yy) * rows
                psnd[c, yy, zz] = part[at : at + rows]
        for s in range(1, ny):
            yy = lax.rem(y + s, ny)
            send(psnd.at[c, yy], prcv.at[c, s - 1], ps_sem, pr_sem.at[c], z * ny + yy, j)

    def then_y(c):
        e = c - late
        take(wrcv.at[e], wr_sem.at[e])
        acc = wsnd[e, z].astype(F32)
        for s in range(1, nz):
            acc = acc + wrcv[e, s - 1].astype(F32)
        vsnd[e] = acc.astype(BF16)
        for s in range(1, ny):
            yy = lax.rem(y + s, ny)
            send(vsnd.at[e, yy], vrcv.at[e, s - 1], es_sem, er_sem.at[e], z * ny + yy, j)

    def then_z(c):
        take(prcv.at[c], pr_sem.at[c])
        acc = psnd[c, y].astype(F32)
        for s in range(1, ny):
            acc = acc + prcv[c, s - 1].astype(F32)
        zsnd[c] = acc.astype(BF16)
        for s in range(1, nz):
            zz = lax.rem(z + s, nz)
            send(zsnd.at[c, zz], zrcv.at[c, s - 1], qs_sem, qr_sem.at[c], zz * ny + y, j)

    def reduced_piece(c):
        if c >= late:
            e = c - late
            take(vrcv.at[e], er_sem.at[e])
            acc = vsnd[e, y].astype(F32)
            for s in range(1, ny):
                acc = acc + vrcv[e, s - 1].astype(F32)
        else:
            take(zrcv.at[c], qr_sem.at[c])
            acc = zsnd[c, z].astype(F32)
            for s in range(1, nz):
                acc = acc + zrcv[c, s - 1].astype(F32)
        return (acc * scale).astype(BF16).astype(F32)

    def reduced(c):
        per = cw // pw
        return jnp.concatenate([reduced_piece(c * per + m) for m in range(per)], axis=1)

    def head_slices(h):
        narrow = pl.ds(pl.multiple_of(h * DK, DK), DK)
        wide = pl.ds(pl.multiple_of(h * DV, DV), DV)
        return narrow, wide

    def state_slice(h, c):
        return pl.ds(pl.multiple_of(h * (DK * DV) + c * DV, DV), DV)

    def read_state(low, high):
        @pl.loop(low, high)
        def _(h):
            narrow, wide = head_slices(h)
            q = query[:, narrow] * decay[:, narrow]
            acc = jnp.zeros((rows, DV), F32)
            for c in range(DK):
                acc = acc + q[:, c : c + 1] * st_ref[:, state_slice(h, c)]
            head[:, wide] = acc

    def write_state(low, high):
        @pl.loop(low, high)
        def _(h):
            narrow, wide = head_slices(h)
            k, d = key[:, narrow], decay[:, narrow]
            v = value[:, wide]
            for c in range(DK):
                at = state_slice(h, c)
                st_ref[:, at] = d[:, c : c + 1] * st_ref[:, at] + k[:, c : c + 1] * v

    for c in range(late, len(pieces)):
        first_z(c)
    for c in range(late):
        first_y(c)
    early = late - 1
    for c in range(early):
        then_z(c)
        if c == late // 2:
            for e in range(late, len(pieces)):
                then_y(e)
    take(ssq.at[pl.ds(0, tp - 1)], sr_sem)
    total = ssq[0]
    for s in range(1, tp):
        total = total + ssq[s]
    scale = lax.rsqrt(total[:, :1] / (kv * width) + epsilon)

    pre = reduced(0) + bias_ref[...]
    log_decay = jnp.minimum(pre, 0.0) - jnp.log1p(jnp.exp(-jnp.abs(pre)))
    decay[...] = jnp.exp(log_decay / decay_normalizer)
    key[...] = reduced(1)
    query[...] = reduced(2) * DK ** (-0.5)
    load_state.wait()
    read_state(0, heads // 2)
    for c in range(early, late):
        then_z(c)
    read_state(heads // 2, heads)
    for c in range(3, 5):
        value[:, (c - 3) * cw : (c - 2) * cw] = reduced(c)
    head_gain = hg_ref[...].astype(F32).reshape(1, DV)
    for h in range(heads):
        at = slice(h * DK, (h + 1) * DK)
        weight = jnp.sum(query[:, at] * key[:, at], axis=1, keepdims=True)
        at = slice(h * DV, (h + 1) * DV)
        acc = head[:, at] + weight * value[:, at]
        acc = acc * lax.rsqrt(jnp.mean(acc * acc, axis=1, keepdims=True) + epsilon)
        head[:, at] = acc * head_gain

    for c in range(5, 7):
        at = slice((c - 5) * cw, (c - 4) * cw)
        both = head[:, at] * jax.nn.silu(reduced(c))
        for p in range(2):
            mixed[p, :, at] = both[p * eight : (p + 1) * eight].astype(BF16)

    for p in range(2):
        for s in range(1, kv):
            k = lax.rem(i + s, kv)
            send(mixed.at[p], mall.at[p, i], ms_sem, mr_sem.at[p], k, j)
    for p in range(2):
        mall[p, i] = mixed[p]
    write_state(0, heads // 4)

    loads[5].wait()
    tokens = kv * eight
    for p in range(2):
        take(mall.at[p, pl.ds(0, kv - 1)], mr_sem.at[p])
        every = mall[p].astype(F32).reshape(tokens, mall.shape[3]).astype(BF16)
        asend[p] = dot(every, vo[...]).astype(BF16).reshape(asend.shape[1:])
        for s in range(1, tp):
            t = lax.rem(j + s, tp)
            send(asend.at[p, t], arecv.at[p, s - 1], as_sem, ar_sem.at[p], i, t)
    slot = lax.rem(i, ratio)
    place = slot * tp + j
    mine = xbuf[pl.ds(j * ratio, ratio)].astype(F32)
    for p in range(2):
        take(arecv.at[p], ar_sem.at[p])
        attn = asend[p, j].astype(F32)
        for s in range(1, tp):
            attn = attn + arecv[p, s - 1].astype(F32)
        part = mine[:, p * eight : (p + 1) * eight].reshape(ratio * eight, width)
        rpart[p] = (part + attn.astype(BF16).astype(F32)).astype(BF16)
        for s in range(kv):
            k = lax.rem(i + s, kv)
            copy = remote(rpart.at[p], rall.at[p, place], rs_sem, rr_sem.at[p], k, owner)
            if s:
                copy.start()
            else:
                pl.when(owner != j)(copy.start)

    @pl.when(owner == j)
    def _():
        for p in range(2):
            rall[p, place] = rpart[p]

    write_state(heads // 4, heads // 2)
    loads[6].wait()
    mlp_gain = mg_ref[...].astype(F32).reshape(1, columns)

    def gathered(p):
        pl.when(owner == j)(lambda: take(rall.at[p, pl.ds(0, kv - 1)], rr_sem.at[p]))
        pl.when(owner != j)(lambda: take(rall.at[p], rr_sem.at[p]))
        return jnp.concatenate(
            [
                (
                    rall[p, a * tp : (a + 1) * tp].reshape(tokens, width).astype(F32)
                    * mlp_gain[:, a * width : (a + 1) * width]
                ).astype(BF16)
                for a in range(ratio)
            ],
            axis=1,
        )

    def own(p, a):
        group = rall[p, a * tp + owner].astype(F32)
        value = group[:eight]
        for m in range(1, ratio):
            value = jnp.where(slot == m, group[m * eight : (m + 1) * eight], value)
        return value

    half = vu.shape[1] // 2
    chunks = usend.shape[1]
    piece = half // chunks

    def columns_of(h, c):
        return pl.ds(pl.multiple_of(h * half + c * piece, 128), piece)

    def up(p, x):
        def give(c):
            usend[p, c] = dot(x, vu[:, columns_of(other, c)]).astype(BF16)
            send(usend.at[p, c], urecv.at[p, c], us_sem, ur_sem.at[p, c], i, partner)

        give(0)
        for c in range(chunks):
            if c + 1 < chunks:
                give(c + 1)
            mine = dot(x, vu[:, columns_of(core, c)])
            take(urecv.at[p, c], ur_sem.at[p, c])
            xsend[p, c] = (mine + urecv[p, c].astype(F32)).astype(BF16)
            for s in range(1, tp // 2):
                to = lax.rem(across + s, tp // 2)
                send(
                    xsend.at[p, c], xrecv.at[p, c, s - 1], xs_sem, xr_sem.at[p, c],
                    i, to * 2 + core,
                )

    def down(p):
        acc = None
        for c in range(chunks):
            take(xrecv.at[p, c], xr_sem.at[p, c])
            total = xsend[p, c].astype(F32)
            for s in range(1, tp // 2):
                total = total + xrecv[p, c, s - 1].astype(F32)
            act[p, 0, c] = jnp.square(jnp.maximum(total, 0.0)).astype(BF16)
            send(act.at[p, 0, c], act.at[p, 1, c], cs_sem, cr_sem.at[p, c], i, partner)
            term = dot(act[p, 0, c], vdn[columns_of(core, c), :])
            acc = term if acc is None else acc + term
        for c in range(chunks):
            take(act.at[p, 1, c], cr_sem.at[p, c])
            acc = acc + dot(act[p, 1, c], vdn[columns_of(other, c), :])
        dsend[p] = acc.reshape(kv, eight, columns).astype(BF16)
        for s in range(1, kv):
            k = lax.rem(i + s, kv)
            send(dsend.at[p, k], drecv.at[p, s - 1], ds_sem, dr_sem.at[p], k, j)

    x0 = gathered(0)
    up(0, x0)
    x1 = gathered(1)
    squares = []
    for p in range(2):
        terms = [own(p, a) for a in range(ratio)]
        squares.append(sum(jnp.sum(term * term, axis=1, keepdims=True) for term in terms))
    squares = jnp.concatenate(squares, axis=0)
    ssq2[j] = jnp.broadcast_to(squares, (rows, 128))
    for s in range(1, tp):
        send(ssq2.at[j], ssq2.at[j], ts_sem, tr_sem, i, lax.rem(j + s, tp))
    up(1, x1)
    loads[7].wait()
    down(0)
    down(1)
    write_state(heads // 2, heads)

    take(ssq2.at[pl.ds(0, tp - 1)], tr_sem)
    squares = ssq2[0]
    for s in range(1, tp):
        squares = squares + ssq2[s]
    scale2 = lax.rsqrt(squares[:, :1] / (columns * tp) + epsilon)
    lines = []
    for p in range(2):
        take(drecv.at[p], dr_sem.at[p])
        acc = dsend[p, i].astype(F32)
        for s in range(1, kv):
            acc = acc + drecv[p, s - 1].astype(F32)
        part = scale2[p * eight : (p + 1) * eight]
        acc = (acc * (part * part)).astype(BF16).astype(F32)
        base = jnp.concatenate([own(p, a) for a in range(ratio)], axis=1)
        lines.append(base + acc)
    out_ref[...] = jnp.concatenate(lines, axis=0).astype(BF16)

    here = jnp.logical_and(owner == j, side == core)
    pl.when(here)(lambda: drain(xbuf.at[pl.ds(0, kv // 2 - 1)], hs_sem))
    pl.when(jnp.logical_not(here))(lambda: drain(xbuf.at[pl.ds(0, kv // 2)], hs_sem))
    drain(xbuf.at[pl.ds(0, kv // 2)], fs_sem)
    drain(ssq.at[pl.ds(0, tp - 1)], ss_sem)
    drain(prcv, ps_sem)
    drain(zrcv, qs_sem)
    drain(wrcv, ws_sem)
    drain(vrcv, es_sem)
    drain(mall.at[:, pl.ds(0, kv - 1)], ms_sem)
    drain(arecv, as_sem)
    pl.when(owner == j)(lambda: drain(rall.at[:, pl.ds(0, kv - 1)], rs_sem))
    pl.when(owner != j)(lambda: drain(rall, rs_sem))
    drain(ssq2.at[pl.ds(0, tp - 1)], ts_sem)
    drain(usend, us_sem)
    drain(xrecv, xs_sem)
    drain(act.at[:, 0], cs_sem)
    drain(drecv, ds_sem)


def layer(
    kv, tp, hidden_rows, carried, norm_gain, weights, decay_bias, head_gain, w_out, mlp_gain,
    w_up, w_down,
):
    rows, columns = hidden_rows.shape
    width = w_out.shape[1]
    ratio = kv // tp
    ny = inner_size(kv)
    nz = kv // ny
    cw = weights[0].shape[1]
    wide = weights[3].shape[1]
    pw = cw // SPLIT
    pieces = sum(w.shape[1] for w in weights) // pw
    late = LATE
    half = w_up.shape[1] // 2
    eight = rows // 2
    tokens = kv * eight
    chunks = max(1, min(CHUNKS, half // 128))
    piece = half // chunks
    limit = VMEM_BYTES - 4 * carried.size - 128 * 1024
    vmem = pl.BlockSpec(memory_space=pltpu.VMEM)
    hbm = pl.BlockSpec(memory_space=pltpu.HBM)
    dma = pltpu.SemaphoreType.DMA
    wq, wk, wd_, wv, wg = weights
    bias = decay_bias.reshape(1, -1)
    return pl.pallas_call(
        functools.partial(layer_kernel, kv, tp),
        out_shape=[
            pltpu.VMEM((rows, columns), BF16),
            pltpu.VMEM(carried.shape, F32),
        ],
        in_specs=[hbm] * 14,
        out_specs=[vmem, vmem],
        scratch_shapes=[
            pltpu.VMEM(a.shape, a.dtype)
            for a in (hidden_rows, norm_gain, bias, head_gain, mlp_gain)
        ]
        + [pltpu.VMEM((1, norm_gain.shape[0]), F32)]
        + [
            pltpu.VMEM(w.shape, BF16) for w in (wq, wk, wd_, wv, wg, w_out, w_up, w_down)
        ]
        + [
            pltpu.VMEM((kv, rows, width), BF16),
            pltpu.VMEM((pieces - late, ny, nz, rows, pw), BF16),
            pltpu.VMEM((pieces - late, ny - 1, nz, rows, pw), BF16),
            pltpu.VMEM((pieces - late, nz, rows, pw), BF16),
            pltpu.VMEM((pieces - late, nz - 1, rows, pw), BF16),
            pltpu.VMEM((late, nz, ny, rows, pw), BF16),
            pltpu.VMEM((late, nz - 1, ny, rows, pw), BF16),
            pltpu.VMEM((late, ny, rows, pw), BF16),
            pltpu.VMEM((late, ny - 1, rows, pw), BF16),
            pltpu.VMEM((tp, rows, 128), F32),
            pltpu.VMEM((rows, cw), F32),
            pltpu.VMEM((rows, cw), F32),
            pltpu.VMEM((rows, cw), F32),
            pltpu.VMEM((rows, wide), F32),
            pltpu.VMEM((rows, wide), F32),
            pltpu.VMEM((2, eight, wide), BF16),
            pltpu.VMEM((2, kv, eight, wide), BF16),
            pltpu.VMEM((2, tp, ratio * eight, width), BF16),
            pltpu.VMEM((2, tp - 1, ratio * eight, width), BF16),
            pltpu.VMEM((2, ratio * eight, width), BF16),
            pltpu.VMEM((2, kv, ratio * eight, width), BF16),
            pltpu.VMEM((2, chunks, tokens, piece), BF16),
            pltpu.VMEM((2, chunks, tokens, piece), BF16),
            pltpu.VMEM((2, chunks, tokens, piece), BF16),
            pltpu.VMEM((2, chunks, tp // 2 - 1, tokens, piece), BF16),
            pltpu.VMEM((2, 2, chunks, tokens, piece), BF16),
            pltpu.VMEM((2, kv, eight, columns), BF16),
            pltpu.VMEM((2, kv - 1, eight, columns), BF16),
            pltpu.VMEM((tp, rows, 128), F32),
            dma((5,)),
            dma((8,)),
            dma((kv // 2,)),
            dma((pieces - late,)),
            dma((pieces - late,)),
            dma((late,)),
            dma((late,)),
            dma((2,)),
            dma((2,)),
            dma((2,)),
            dma((2, chunks)),
            dma((2, chunks)),
            dma((2, chunks)),
            dma((2,)),
            dma((ONES,)),
        ],
        compiler_params=pltpu.CompilerParams(
            has_side_effects=True, collective_id=0, vmem_limit_bytes=limit
        ),
        name="layer",
    )(
        hidden_rows, norm_gain, bias, head_gain, mlp_gain, wq, wk, wd_, wv, wg, carried,
        w_out, w_up, w_down,
    )


def store_kernel(parts, new_in, rows_in, new_out, rows_out, sems):
    size = new_in.shape[1] // parts
    copies = [pltpu.make_async_copy(rows_in, rows_out, sems.at[parts])]
    for n in range(parts):
        at = pl.ds(n * size, size)
        copies.append(pltpu.make_async_copy(new_in.at[:, at], new_out.at[:, at], sems.at[n]))
    for copy in copies:
        copy.start()
    for copy in copies:
        copy.wait()


def store(updated_rows, new_state):
    parts = STORES
    vmem = pl.BlockSpec(memory_space=pltpu.VMEM)
    hbm = pl.BlockSpec(memory_space=pltpu.HBM)
    return pl.pallas_call(
        functools.partial(store_kernel, parts),
        out_shape=[
            jax.ShapeDtypeStruct(new_state.shape, new_state.dtype),
            jax.ShapeDtypeStruct(updated_rows.shape, updated_rows.dtype),
        ],
        in_specs=[vmem, vmem],
        out_specs=[hbm, hbm],
        scratch_shapes=[pltpu.SemaphoreType.DMA((parts + 1,))],
        compiler_params=pltpu.CompilerParams(vmem_limit_bytes=1024 * 1024),
        name="store",
    )(new_state, updated_rows)


def body(
    kv,
    tp,
    hidden_rows,
    carried_state,
    norm_gain,
    w_query,
    w_key,
    w_decay,
    w_value,
    w_gate,
    decay_bias,
    head_gain,
    w_out,
    mlp_gain,
    w_up,
    w_down,
):
    updated_rows, new_state = layer(
        kv, tp, hidden_rows, carried_state, norm_gain,
        (w_query, w_key, w_decay, w_value, w_gate), decay_bias, head_gain, w_out, mlp_gain,
        w_up, w_down,
    )
    new_state, updated_rows = store(updated_rows, new_state)
    return (updated_rows, new_state)


def solution(mesh):
    return jax.shard_map(
        functools.partial(body, mesh.shape["kv"], mesh.shape["tp"]),
        mesh=mesh,
        in_specs=(
            P("kv", "tp"),
            P("kv", "tp"),
            P(),
            P("kv", "tp"),
            P("kv", "tp"),
            P("kv", "tp"),
            P("kv", "tp"),
            P("kv", "tp"),
            P("tp"),
            P(),
            P("tp", "kv"),
            P("tp"),
            P("tp", "kv"),
            P("kv", "tp"),
        ),
        out_specs=(P("kv", "tp"), P("kv", "tp")),
        check_vma=False,
    )
```

time: 65 us -> 61.7 us (0.949); the launches traced: 63.9 us -> 61.5 us
  Pallas kernels: 63.2 us -> 60.9 us
    pallas_call x1, Pallas kernels: 59.9 us -> 57.5 us  [layer(): pl.pallas_call(functools.partial(layer_kernel, kv, tp), out_shape=[pltpu....]
where the time goes in v3:
time: 61.7 us; the launch traced here: 61.5 us
  Pallas kernels  60.9 us (99%)
  between operations  0.64 us (1%)
    pallas_call x1, Pallas kernels, layer(): pl.pallas_call(functools.partial(layer_kernel, kv, tp), out_shape=[pltpu....  57.5 us
    pallas_call x1, Pallas kernels, store(): pl.pallas_call(functools.partial(store_kernel, parts), out_shape=[jax.Sha...  3.39 us

profile of v3, /device:TPU:0, one launch (start us, length us, event | category | flops | bytes accessed | tf_op | source)
XLA Modules:
  0.0 61.5 jit_solution(2175123690863423278)
XLA Ops:
  0.6 57.5 %layer.1 = (bf16[16,1024]{1,0:T(8,128)(2,1)S(1)}, f32[16,131072]{1,0:T(8,128)S(1)}) custom-call(bf16[16,1024]{1,0:T(8,128)(2,1)} %h_in.1, bf16[4096]{0:T(1024)(128)(2,1)} %ng_in.1, f32[1,512]{1,0:T(1,128)} %bitcast.1, bf16[256]{0:T(256)(128)(2,1)} %hg_in.1, bf16[1024]{0:T(1024)(128)(2,1)} %mg_in.1, bf16[512,512]{1,0:T(8,128)(2,1)} %wq.1, ...), custom_call_target="tpu_custom_call" | custom-call | tf_op jit(solution)/shard_map/layer/pallas_call | solution.py:510
  58.1 3.4 %store.1 = (f32[16,131072]{1,0:T(8,128)}, bf16[16,1024]{1,0:T(8,128)(2,1)}) custom-call(f32[16,131072]{1,0:T(8,128)S(1)} %get-tuple-element.6.new_in, bf16[16,1024]{1,0:T(8,128)(2,1)S(1)} %get-tuple-element.7.rows_in), custom_call_target="tpu_custom_call" | custom-call | tf_op jit(solution)/shard_map/store/pallas_call | solution.py:598

commit v4 on v3

--- a/solution.py
+++ b/solution.py
@@ -275,16 +275,16 @@
                 at = state_slice(h, c)
                 st_ref[:, at] = d[:, c : c + 1] * st_ref[:, at] + k[:, c : c + 1] * v
 
+    first_y(0)
     for c in range(late, len(pieces)):
         first_z(c)
+    for c in range(1, late):
+        first_y(c)
     for c in range(late):
-        first_y(c)
-    early = late - 1
-    for c in range(early):
-        then_z(c)
-        if c == late // 2:
+        if c == late - 1:
             for e in range(late, len(pieces)):
                 then_y(e)
+        then_z(c)
     take(ssq.at[pl.ds(0, tp - 1)], sr_sem)
     total = ssq[0]
     for s in range(1, tp):
@@ -297,10 +297,7 @@
     key[...] = reduced(1)
     query[...] = reduced(2) * DK ** (-0.5)
     load_state.wait()
-    read_state(0, heads // 2)
-    for c in range(early, late):
-        then_z(c)
-    read_state(heads // 2, heads)
+    read_state(0, heads)
     for c in range(3, 5):
         value[:, (c - 3) * cw : (c - 2) * cw] = reduced(c)
     head_gain = hg_ref[...].astype(F32).reshape(1, DV)
@@ -324,7 +321,7 @@
             send(mixed.at[p], mall.at[p, i], ms_sem, mr_sem.at[p], k, j)
     for p in range(2):
         mall[p, i] = mixed[p]
-    write_state(0, heads // 4)
+    write_state(0, heads // 2)
 
     loads[5].wait()
     tokens = kv * eight
@@ -358,7 +355,6 @@
         for p in range(2):
             rall[p, place] = rpart[p]
 
-    write_state(heads // 4, heads // 2)
     loads[6].wait()
     mlp_gain = mg_ref[...].astype(F32).reshape(1, columns)
 
@@ -431,6 +427,7 @@
     x0 = gathered(0)
     up(0, x0)
     x1 = gathered(1)
+    up(1, x1)
     squares = []
     for p in range(2):
         terms = [own(p, a) for a in range(ratio)]
@@ -439,7 +436,6 @@
     ssq2[j] = jnp.broadcast_to(squares, (rows, 128))
     for s in range(1, tp):
         send(ssq2.at[j], ssq2.at[j], ts_sem, tr_sem, i, lax.rem(j + s, tp))
-    up(1, x1)
     loads[7].wait()
     down(0)
     down(1)

time: 61.7 us -> 61.1 us (level)
  no operation moved by 1% of the time
where the time goes in v4:
time: 61.1 us; the launch traced here: 60.9 us
  Pallas kernels  60.3 us (99%)
  between operations  0.64 us (1%)
    pallas_call x1, Pallas kernels, layer(): pl.pallas_call(functools.partial(layer_kernel, kv, tp), out_shape=[pltpu....  56.9 us
    pallas_call x1, Pallas kernels, store(): pl.pallas_call(functools.partial(store_kernel, parts), out_shape=[jax.Sha...  3.39 us

profile of v4, /device:TPU:0, one launch (start us, length us, event | category | flops | bytes accessed | tf_op | source)
XLA Modules:
  0.0 60.9 jit_solution(8799566231822047318)
XLA Ops:
  0.6 56.9 %layer.1 = (bf16[16,1024]{1,0:T(8,128)(2,1)S(1)}, f32[16,131072]{1,0:T(8,128)S(1)}) custom-call(bf16[16,1024]{1,0:T(8,128)(2,1)} %h_in.1, bf16[4096]{0:T(1024)(128)(2,1)} %ng_in.1, f32[1,512]{1,0:T(1,128)} %bitcast.1, bf16[256]{0:T(256)(128)(2,1)} %hg_in.1, bf16[1024]{0:T(1024)(128)(2,1)} %mg_in.1, bf16[512,512]{1,0:T(8,128)(2,1)} %wq.1, ...), custom_call_target="tpu_custom_call" | custom-call | tf_op jit(solution)/shard_map/layer/pallas_call | solution.py:506
  57.5 3.4 %store.1 = (f32[16,131072]{1,0:T(8,128)}, bf16[16,1024]{1,0:T(8,128)(2,1)}) custom-call(f32[16,131072]{1,0:T(8,128)S(1)} %get-tuple-element.6.new_in, bf16[16,1024]{1,0:T(8,128)(2,1)S(1)} %get-tuple-element.7.rows_in), custom_call_target="tpu_custom_call" | custom-call | tf_op jit(solution)/shard_map/store/pallas_call | solution.py:594

commit v5 on v4

--- a/solution.py
+++ b/solution.py
@@ -88,6 +88,23 @@
     def send(src, dst, send_sem, recv_sem, a, b):
         remote(src, dst, send_sem, recv_sem, a, b).start()
 
+    upward = z < nz // 2
+    far_z = [jnp.where(upward, n, nz - 1 - n) for n in range(nz)]
+
+    def along_line(send_to):
+        for zz in far_z:
+            pl.when(zz != z)(functools.partial(send_to, zz, lax.rem(zz - z + nz, nz) - 1))
+
+    def along_plane(send_to):
+        for zz in far_z:
+            for u in range(ny):
+                k = zz * ny + lax.rem(y + u, ny)
+                call = functools.partial(send_to, k, lax.rem(k - i + kv, kv) - 1)
+                if u:
+                    call()
+                else:
+                    pl.when(k != i)(call)
+
     inputs = [
         pltpu.make_async_copy(src, dst, insem.at[n])
         for n, (src, dst) in enumerate(
@@ -194,9 +211,11 @@
             for yy in range(ny):
                 at = (zz * ny + yy) * rows
                 wsnd[e, zz, yy] = part[at : at + rows]
-        for s in range(1, nz):
-            zz = lax.rem(z + s, nz)
-            send(wsnd.at[e, zz], wrcv.at[e, s - 1], ws_sem, wr_sem.at[e], zz * ny + y, j)
+        along_line(
+            lambda zz, to: send(
+                wsnd.at[e, zz], wrcv.at[e, to], ws_sem, wr_sem.at[e], zz * ny + y, j
+            )
+        )
 
     def first_y(c):
         part = product(c)
@@ -225,9 +244,11 @@
         for s in range(1, ny):
             acc = acc + prcv[c, s - 1].astype(F32)
         zsnd[c] = acc.astype(BF16)
-        for s in range(1, nz):
-            zz = lax.rem(z + s, nz)
-            send(zsnd.at[c, zz], zrcv.at[c, s - 1], qs_sem, qr_sem.at[c], zz * ny + y, j)
+        along_line(
+            lambda zz, to: send(
+                zsnd.at[c, zz], zrcv.at[c, to], qs_sem, qr_sem.at[c], zz * ny + y, j
+            )
+        )
 
     def reduced_piece(c):
         if c >= late:
@@ -316,9 +337,9 @@
             mixed[p, :, at] = both[p * eight : (p + 1) * eight].astype(BF16)
 
     for p in range(2):
-        for s in range(1, kv):
-            k = lax.rem(i + s, kv)
-            send(mixed.at[p], mall.at[p, i], ms_sem, mr_sem.at[p], k, j)
+        along_plane(
+            lambda k, to: send(mixed.at[p], mall.at[p, i], ms_sem, mr_sem.at[p], k, j)
+        )
     for p in range(2):
         mall[p, i] = mixed[p]
     write_state(0, heads // 2)
@@ -342,13 +363,11 @@
             attn = attn + arecv[p, s - 1].astype(F32)
         part = mine[:, p * eight : (p + 1) * eight].reshape(ratio * eight, width)
         rpart[p] = (part + attn.astype(BF16).astype(F32)).astype(BF16)
-        for s in range(kv):
-            k = lax.rem(i + s, kv)
-            copy = remote(rpart.at[p], rall.at[p, place], rs_sem, rr_sem.at[p], k, owner)
-            if s:
-                copy.start()
-            else:
-                pl.when(owner != j)(copy.start)
+        give = lambda k, to: send(
+            rpart.at[p], rall.at[p, place], rs_sem, rr_sem.at[p], k, owner
+        )
+        along_plane(give)
+        pl.when(owner != j)(lambda: give(i, 0))
 
     @pl.when(owner == j)
     def _():
@@ -420,9 +439,9 @@
             take(act.at[p, 1, c], cr_sem.at[p, c])
             acc = acc + dot(act[p, 1, c], vdn[columns_of(other, c), :])
         dsend[p] = acc.reshape(kv, eight, columns).astype(BF16)
-        for s in range(1, kv):
-            k = lax.rem(i + s, kv)
-            send(dsend.at[p, k], drecv.at[p, s - 1], ds_sem, dr_sem.at[p], k, j)
+        along_plane(
+            lambda k, to: send(dsend.at[p, k], drecv.at[p, to], ds_sem, dr_sem.at[p], k, j)
+        )
 
     x0 = gathered(0)
     up(0, x0)

time: 61.1 us -> 60.9 us (level)
  no operation moved by 1% of the time
where the time goes in v5:
time: 60.9 us; the launch traced here: 60.8 us
  Pallas kernels  60.1 us (99%)
  between operations  0.64 us (1%)
    pallas_call x1, Pallas kernels, layer(): pl.pallas_call(functools.partial(layer_kernel, kv, tp), out_shape=[pltpu....  56.7 us
    pallas_call x1, Pallas kernels, store(): pl.pallas_call(functools.partial(store_kernel, parts), out_shape=[jax.Sha...  3.39 us

profile of v5, /device:TPU:0, one launch (start us, length us, event | category | flops | bytes accessed | tf_op | source)
XLA Modules:
  0.0 60.8 jit_solution(9755807253889661500)
XLA Ops:
  0.6 56.7 %layer.1 = (bf16[16,1024]{1,0:T(8,128)(2,1)S(1)}, f32[16,131072]{1,0:T(8,128)S(1)}) custom-call(bf16[16,1024]{1,0:T(8,128)(2,1)} %h_in.1, bf16[4096]{0:T(1024)(128)(2,1)} %ng_in.1, f32[1,512]{1,0:T(1,128)} %bitcast.1, bf16[256]{0:T(256)(128)(2,1)} %hg_in.1, bf16[1024]{0:T(1024)(128)(2,1)} %mg_in.1, bf16[512,512]{1,0:T(8,128)(2,1)} %wq.1, ...), custom_call_target="tpu_custom_call" | custom-call | tf_op jit(solution)/shard_map/layer/pallas_call | solution.py:525
  57.4 3.4 %store.1 = (f32[16,131072]{1,0:T(8,128)}, bf16[16,1024]{1,0:T(8,128)(2,1)}) custom-call(f32[16,131072]{1,0:T(8,128)S(1)} %get-tuple-element.6.new_in, bf16[16,1024]{1,0:T(8,128)(2,1)S(1)} %get-tuple-element.7.rows_in), custom_call_target="tpu_custom_call" | custom-call | tf_op jit(solution)/shard_map/store/pallas_call | solution.py:613
